TPU v7x, 32 devices: a whole 2x2x4 slice. The times are simulated.
32 devices in a mesh: ep: 8 (over z, core), tp: 4 (over y, x).
Axes of the slice: x: 2, y: 2, z: 4, core: 2. Of those that a mesh axis runs over, the one named last changes fastest.
Arguments:
- mixer_input: bfloat16 [2048, 2048], P('ep'), may hold values from -6 to 6
- mixer_gain: float32 [2048], replicated, may hold values from 0.1 to 1.9
- query_weight: bfloat16 [2048, 2048], P(None, 'tp'), may hold values from -0.13258252 to 0.13258252
- key_weight: bfloat16 [2048, 1024], P(None, 'tp'), may hold values from -2.78423295 to 2.78423295
- value_weight: bfloat16 [2048, 1024], P(None, 'tp'), may hold values from -0.125 to 0.125
- output_weight: bfloat16 [2048, 2048], P(None, 'tp'), may hold values from -1 to 1
- sink_logit: float32 [32], P('tp'), may hold values from 2 to 7
- expert_input: bfloat16 [1024, 2048], P('ep'), may hold values from -6 to 6
- expert_gain: float32 [2048], replicated, may hold values from 0.1 to 1.9
- routes: int32 [1024, 4], P('ep'), may hold values from 0 to 7, all different within a row; in each aligned block of 128 rows (0 to 127, 128 to 255, ...) at most 128 rows name the same one
- route_logits: float32 [1024, 4], P('ep'), may hold values from -6 to 6
- gate_weight: bfloat16 [8, 2048, 2048], P('ep', None, 'tp'), may hold values from -0.375 to 0.375
- up_weight: bfloat16 [8, 2048, 2048], P('ep', None, 'tp'), may hold values from -0.375 to 0.375
- down_weight: bfloat16 [8, 2048, 2048], P('ep', None, 'tp'), may hold values from -0.03125 to 0.03125
Outputs:
- mixer_output: bfloat16 [2048, 2048], P('ep', 'tp')
- expert_output: bfloat16 [1024, 2048], P('ep', 'tp')
Inputs may be any that keep to these rules, and one draw needn't show every extreme that they name: `routes`: each token names 4 different experts. Among the 128 tokens of one index of ep (aligned blocks) no expert is named more than 128 times, and in some blocks one expert is named exactly 128 times.
All inputs are finite; a program needn't handle non-finite values.
Results may differ from a plain program's by a relative error of at most 0.0055.
The roundings to bfloat16 on the way count: a program that leaves them out, or rounds other values in their place, can miss the bound.
Values may be sent and summed in bfloat16 or wider, within the bound.
A program may use at most 64 MiB of HBM per device.

v0:
```python
import functools

import jax
import jax.numpy as jnp
from jax import lax
from jax.experimental import pallas as pl
from jax.experimental.pallas import tpu as pltpu
from jax.sharding import PartitionSpec as P

HEAD_DIM = 64
TOP_K = 4
WINDOW = 128
GRID_W = 64


EPSILON = 1e-06
LIMIT = 7.0
SLOPE = 1.702
BASE = 10000.0


def normalize(rows, gain):
    values = rows.astype(jnp.float32)
    scaled = values * lax.rsqrt(jnp.mean(values * values, axis=-1, keepdims=True) + EPSILON)
    return (scaled * gain).astype(jnp.bfloat16)


def rotate(values, cosine, sine):
    width = values.shape[1]
    lanes = cosine.shape[1]
    if width < lanes:
        return rotate(jnp.concatenate([values] * (lanes // width), axis=1), cosine, sine)[:, :width]
    spot = lax.broadcasted_iota(jnp.int32, cosine.shape, 1)
    leading = spot % (HEAD_DIM // 2) < HEAD_DIM // 4
    pieces = []
    for start in range(0, width, lanes):
        piece = values[:, start : start + lanes]
        other = jnp.where(
            leading,
            pltpu.roll(piece, lanes - HEAD_DIM // 4, 1),
            pltpu.roll(piece, HEAD_DIM // 4, 1),
        )
        pieces.append(piece * cosine + other * sine)
    return jnp.concatenate(pieces, axis=1)


def activate(gate, up):
    capped = jnp.minimum(gate, LIMIT)
    bounded = jnp.clip(up, -LIMIT, LIMIT)
    return (capped * jax.nn.sigmoid(SLOPE * capped) * (bounded + 1.0)).astype(jnp.bfloat16)


def remote(src, dst, sent, landed, ep, tp):
    return pltpu.make_async_remote_copy(
        src_ref=src,
        dst_ref=dst,
        send_sem=sent,
        recv_sem=landed,
        device_id=(ep, tp),
        device_id_type=pl.DeviceIdType.MESH,
    )


def exchange(
    n,
    t,
    x_ref,
    gain_ref,
    share_ref,
    mixer_ref,
    mixer_gain_ref,
    cosine_ref,
    sine_ref,
    sink_ref,
    wq_hbm,
    wk_hbm,
    wv_hbm,
    wo_hbm,
    wg_hbm,
    wu_hbm,
    wd_hbm,
    mixer_out,
    expert_out,
    tokens,
    hidden,
    heads,
    result,
    returned,
    queries,
    around,
    wq,
    wk,
    wv,
    wo,
    wg,
    wu,
    wd,
    local_sem,
    token_recv,
    far_send,
    near_send,
    core_send,
    hidden_send,
    hidden_recv,
    pass_send,
    pass_recv,
    head_send,
    head_recv,
    edge_send,
    edge_recv,
    result_send,
    result_recv,
):
    ep, tp = lax.axis_index("ep"), lax.axis_index("tp")
    chips = n // 2
    z, core = ep // 2, ep % 2
    step = 1 - 2 * core
    partner = 2 * z + 1 - core
    rows = x_ref.shape[0]
    pair = 2 * rows
    part = wg.shape[1]
    far, near = chips // 2, chips - 1 - chips // 2
    square = t == 4
    direct = (1, 2) if square else tuple(range(1, t))

    def peer(k):
        if not square:
            return lax.rem(tp + k, t)
        return lax.rem(tp + (k // 2) * 2 + (k % 2) * (1 - 2 * (tp % 2)) + t, t)

    def chip(hops):
        return lax.rem(z + hops * step + 2 * chips, chips)

    def block(buffer, index, size):
        return buffer.at[pl.ds(pl.multiple_of(index * size, size), size)]

    loads = [
        pltpu.make_async_copy(a, b, local_sem.at[i])
        for i, (a, b) in enumerate((
            (wq_hbm, wq),
            (wk_hbm, wk),
            (wv_hbm, wv),
            (wg_hbm, wg),
            (wu_hbm, wu),
            (wo_hbm, wo),
            (wd_hbm, wd),
        ))
    ]
    for load in loads:
        load.start()

    barrier = pltpu.get_barrier_semaphore()
    for k in range(1, n):
        pl.semaphore_signal(
            barrier,
            inc=1,
            device_id=(lax.rem(ep + k, n), tp),
            device_id_type=pl.DeviceIdType.MESH,
        )
    for k in range(1, t):
        pl.semaphore_signal(
            barrier,
            inc=1,
            device_id=(ep, peer(k)),
            device_id_type=pl.DeviceIdType.MESH,
        )
    tokens[pl.ds(pl.multiple_of(ep * rows, rows), rows), :] = normalize(x_ref[...], gain_ref[...])
    pl.semaphore_wait(barrier, n + t - 2)

    def token_copy(slot, sent, target):
        piece = block(tokens, slot, rows)
        return remote(piece, piece, sent, token_recv.at[slot], target, tp)

    def forward_far(hop):
        return token_copy(2 * chip(-hop) + core, far_send.at[hop], 2 * chip(1) + core)

    def forward_near(hop):
        return token_copy(2 * chip(hop) + core, near_send.at[hop], 2 * chip(-1) + core)

    def forward_core(hops):
        place = chip(hops)
        return token_copy(2 * place + core, core_send.at[place], partner)

    def token_wait(slot):
        token_copy(slot, core_send.at[0], partner).wait_recv()

    if far > 0:
        forward_far(0).start()
    if near > 0:
        forward_near(0).start()
    forward_core(0).start()

    def head_copy(source, k):
        piece = heads.at[source]
        return remote(piece, piece, head_send.at[k], head_recv.at[source], ep, peer(k))

    def pass_copy(place, way):
        source = peer(2 - way)
        if place is None:
            start, size, index = 0, heads.shape[1] // 2, chips
            buffer = heads.at[source]
        else:
            start, size, index = place * pair, rows, place
            buffer = hidden.at[source]
        piece = buffer.at[pl.ds(pl.multiple_of(start + (1 - way) * size, size), size)]
        return remote(
            piece, piece, pass_send.at[way, index], pass_recv.at[way, index], ep, peer(1 + way)
        )

    def pass_wait(place, way):
        if place is None:
            start, size, index = 0, heads.shape[1] // 2, chips
            buffer = heads.at[peer(3)]
        else:
            start, size, index = place * pair, rows, place
            buffer = hidden.at[peer(3)]
        piece = buffer.at[pl.ds(pl.multiple_of(start + (1 - way) * size, size), size)]
        remote(
            piece, piece, pass_send.at[way, index], pass_recv.at[way, index], ep, peer(1 + way)
        ).wait_recv()

    def hidden_copy(source, place, k):
        piece = block(hidden.at[source], place, pair)
        return remote(
            piece,
            piece,
            hidden_send.at[k, place],
            hidden_recv.at[source, place],
            ep,
            peer(k),
        )

    def hidden_pass(place):
        if square:
            for way in range(2):
                hidden_copy(peer(2 - way), place, 2 - way).wait_recv()
                pass_copy(place, way).start()

    def hidden_wait(place):
        if square:
            for way in range(2):
                pass_wait(place, way)
        else:
            for k in direct:
                hidden_copy(peer(k), place, k).wait_recv()

    def first_half(place):
        token_wait(2 * place + 1 - core)
        inside = pl.ds(pl.multiple_of(place * pair, pair), pair)
        span = min(256, part)
        for start in range(0, part, span):
            cut = slice(start, start + span)
            gate = jnp.dot(tokens[inside, :], wg[:, cut], preferred_element_type=jnp.float32)
            up = jnp.dot(tokens[inside, :], wu[:, cut], preferred_element_type=jnp.float32)
            hidden[tp, inside, cut] = activate(gate, up)
        for k in direct:
            hidden_copy(tp, place, k).start()

    length = mixer_ref.shape[0]
    kept = wk.shape[1]
    normed = normalize(mixer_ref[...], mixer_gain_ref[...])
    cosine, sine = cosine_ref[...], sine_ref[...]
    own = slice(WINDOW, WINDOW + length)
    for load in loads[:3]:
        load.wait()
    keys = jnp.dot(normed, wk[...], preferred_element_type=jnp.float32)
    around[own, 0:kept] = rotate(keys, cosine, sine).astype(jnp.bfloat16)
    around[own, kept:] = jnp.dot(normed, wv[...], preferred_element_type=jnp.float32).astype(
        jnp.bfloat16
    )

    def edge_copy(way):
        source, target = (length, 0) if way == 0 else (WINDOW, WINDOW + length)
        return remote(
            around.at[pl.ds(source, WINDOW)],
            around.at[pl.ds(target, WINDOW)],
            edge_send.at[way],
            edge_recv.at[way],
            lax.rem(ep + (1 if way == 0 else n - 1), n),
            tp,
        )

    for way in range(2):
        edge_copy(way).start()
    turned = jnp.dot(normed, wq[...], preferred_element_type=jnp.float32)
    queries[...] = rotate(turned, cosine, sine).astype(jnp.bfloat16)

    loads[3].wait()
    loads[4].wait()
    first_half(z)

    def attend(number, carry):
        inside = pl.ds(pl.multiple_of(number * WINDOW, WINDOW), WINDOW)
        seen = pl.ds(pl.multiple_of(number * WINDOW, WINDOW), 3 * WINDOW)
        shape = (WINDOW, 3 * WINDOW)
        line = lax.broadcasted_iota(jnp.int32, shape, 0)
        key = lax.broadcasted_iota(jnp.int32, shape, 1)
        place = ep * length + (number - 1) * WINDOW + key
        allowed = (key >= line) & (key <= line + 2 * WINDOW) & (place >= 0) & (place < n * length)
        group = queries.shape[1] // kept
        allowed = jnp.concatenate([allowed] * group, axis=0)
        for head in range(kept // HEAD_DIM):
            first = head * group
            query = jnp.concatenate(
                [
                    queries[inside, (first + r) * HEAD_DIM : (first + r + 1) * HEAD_DIM]
                    for r in range(group)
                ],
                axis=0,
            )
            sinks = jnp.concatenate(
                [
                    jnp.broadcast_to(sink_ref[:, first + r : first + r + 1], (WINDOW, 1))
                    for r in range(group)
                ],
                axis=0,
            )
            near_keys = around[seen, head * HEAD_DIM : (head + 1) * HEAD_DIM]
            near_values = around[seen, kept + head * HEAD_DIM : kept + (head + 1) * HEAD_DIM]
            scores = lax.dot_general(
                query,
                near_keys,
                (((1,), (1,)), ((), ())),
                preferred_element_type=jnp.float32,
            ) * HEAD_DIM ** (-0.5)
            scores = jnp.where(allowed, scores, -1e30)
            top = jnp.maximum(jnp.max(scores, axis=-1, keepdims=True), sinks)
            weights = jnp.exp(scores - top)
            denominator = jnp.sum(weights, axis=-1, keepdims=True) + jnp.exp(sinks - top)
            shares = (weights * (1.0 / denominator)).astype(jnp.bfloat16)
            mixed = jnp.dot(shares, near_values, preferred_element_type=jnp.float32)
            mixed = mixed.astype(jnp.bfloat16)
            heads[tp, inside, first * HEAD_DIM : (first + group) * HEAD_DIM] = jnp.concatenate(
                [mixed[r * WINDOW : (r + 1) * WINDOW] for r in range(group)], axis=1
            )
        return carry

    def attention():
        for way in range(2):
            edge_copy(way).wait_recv()
        lax.fori_loop(0, length // WINDOW, attend, 0)
        for k in direct:
            head_copy(tp, k).start()

    for hop in range(1, far + 1):
        token_wait(2 * chip(-hop) + core)
        if hop < far:
            forward_far(hop).start()
        forward_core(-hop).start()
        if hop <= near:
            token_wait(2 * chip(hop) + core)
            if hop < near:
                forward_near(hop).start()
            forward_core(hop).start()
            if hop == 1:
                attention()

            def both(k, carry, hop=hop):
                first_half(chip((2 * k - 1) * hop))
                return carry

            lax.fori_loop(0, 2, both, 0)
            if hop == 1 and square:
                hidden_pass(z)
                for way in range(2):
                    head_copy(peer(2 - way), 2 - way).wait_recv()
                    pass_copy(None, way).start()
        else:
            first_half(chip(-hop))

    def place_of(i):
        return chip((i + 1) // 2 * (2 * ((i + 1) % 2) - 1))

    def pass_on(i, carry):
        hidden_pass(place_of(i))
        return carry

    lax.fori_loop(1, chips - 1, pass_on, 0)

    loads[5].wait()
    if square:
        for way in range(2):
            pass_wait(None, way)
    else:
        for k in direct:
            head_copy(peer(k), k).wait_recv()
    total = jnp.dot(heads[0], wo[0:part, :], preferred_element_type=jnp.float32)
    for k in range(1, t):
        total += jnp.dot(
            heads[k], wo[k * part : (k + 1) * part, :], preferred_element_type=jnp.float32
        )
    mixer_out[...] = total.astype(jnp.bfloat16)

    loads[6].wait()

    def result_copy(source, owner):
        return remote(
            block(result, owner, rows),
            returned.at[source],
            result_send.at[owner],
            result_recv.at[source],
            owner,
            tp,
        )

    def second_half(i, carry):
        place = place_of(i)
        inside = pl.ds(pl.multiple_of(place * pair, pair), pair)
        hidden_wait(place)
        total = jnp.dot(hidden[0, inside, :], wd[0:part, :], preferred_element_type=jnp.float32)
        for k in range(1, t):
            total += jnp.dot(
                hidden[k, inside, :],
                wd[k * part : (k + 1) * part, :],
                preferred_element_type=jnp.float32,
            )
        result[inside, :] = total.astype(jnp.bfloat16)

        @pl.when(i == 0)
        def _():
            result_copy(ep, partner).start()
            returned[ep] = result[pl.ds(pl.multiple_of(ep * rows, rows), rows), :]

        @pl.when(i > 0)
        def _():
            result_copy(ep, 2 * place + core).start()
            result_copy(ep, 2 * place + 1 - core).start()

        return carry

    lax.fori_loop(0, chips - 2, second_half, 0)
    hidden_pass(place_of(chips - 1))
    lax.fori_loop(chips - 2, chips, second_half, 0)

    for k in range(1, n):
        other = lax.rem(ep + k, n)
        result_copy(other, other).wait_recv()
    total = returned[0].astype(jnp.float32) * share_ref[:, 0:1]
    for e in range(1, n):
        total += returned[e].astype(jnp.float32) * share_ref[:, e : e + 1]
    expert_out[...] = total.astype(jnp.bfloat16)

    for hop in range(far):
        forward_far(hop).wait_send()
    for hop in range(near):
        forward_near(hop).wait_send()
    for hop in range(chips):
        forward_core(hop).wait_send()
    for way in range(2):
        edge_copy(way).wait_send()
        if square:
            pass_copy(None, way).wait_send()
            for place in range(chips):
                pass_copy(place, way).wait_send()
    for k in direct:
        head_copy(tp, k).wait_send()
        for place in range(chips):
            hidden_copy(tp, place, k).wait_send()
    for k in range(1, n):
        result_copy(ep, lax.rem(ep + k, n)).wait_send()


def shards(
    mixer_input,
    mixer_gain,
    query_weight,
    key_weight,
    value_weight,
    output_weight,
    sink_logit,
    expert_input,
    expert_gain,
    routes,
    route_logits,
    gate_weight,
    up_weight,
    down_weight,
):
    tokens = mixer_input.shape[0]
    lanes = 2 * HEAD_DIM
    quarter = HEAD_DIM // 4
    spot = jnp.arange(lanes, dtype=jnp.int32)[None, :]
    place = (lax.axis_index("ep") * tokens + jnp.arange(tokens, dtype=jnp.int32))[:, None]
    frequency = BASE ** (-(spot % quarter).astype(jnp.float32) / quarter)
    by_row = spot % HEAD_DIM < HEAD_DIM // 2
    turn = jnp.where(by_row, place // GRID_W, place % GRID_W).astype(jnp.float32) * frequency
    cosine = jnp.cos(turn)
    sine = jnp.sin(turn) * jnp.where(spot % (HEAD_DIM // 2) < quarter, -1.0, 1.0)
    experts = lax.axis_size("ep")
    parts = lax.axis_size("tp")
    rows_here, width = expert_input.shape
    part = gate_weight.shape[2]
    chances = jax.nn.softmax(route_logits, axis=-1)
    named = routes[:, :, None] == jnp.arange(experts, dtype=jnp.int32)[None, None, :]
    expert_share = jnp.sum(jnp.where(named, chances[:, :, None], 0.0), axis=1)
    vmem = pl.BlockSpec(memory_space=pltpu.VMEM)
    anywhere = pl.BlockSpec(memory_space=pl.ANY)
    chips = experts // 2
    dma = pltpu.SemaphoreType.DMA
    columns = down_weight.shape[2]
    return pl.pallas_call(
        functools.partial(exchange, experts, parts),
        out_shape=(
            jax.ShapeDtypeStruct((tokens, output_weight.shape[1]), jnp.bfloat16),
            jax.ShapeDtypeStruct((rows_here, columns), jnp.bfloat16),
        ),
        in_specs=[vmem] * 8 + [anywhere] * 7,
        out_specs=(vmem, vmem),
        scratch_shapes=[
            pltpu.VMEM((experts * rows_here, width), jnp.bfloat16),
            pltpu.VMEM((parts, experts * rows_here, part), jnp.bfloat16),
            pltpu.VMEM((parts, tokens, query_weight.shape[1]), jnp.bfloat16),
            pltpu.VMEM((experts * rows_here, columns), jnp.bfloat16),
            pltpu.VMEM((experts, rows_here, columns), jnp.bfloat16),
            pltpu.VMEM((tokens, query_weight.shape[1]), jnp.bfloat16),
            pltpu.VMEM((tokens + 2 * WINDOW, 2 * key_weight.shape[1]), jnp.bfloat16),
            pltpu.VMEM(query_weight.shape, jnp.bfloat16),
            pltpu.VMEM(key_weight.shape, jnp.bfloat16),
            pltpu.VMEM(value_weight.shape, jnp.bfloat16),
            pltpu.VMEM(output_weight.shape, jnp.bfloat16),
            pltpu.VMEM(gate_weight.shape[1:], jnp.bfloat16),
            pltpu.VMEM(up_weight.shape[1:], jnp.bfloat16),
            pltpu.VMEM(down_weight.shape[1:], jnp.bfloat16),
            dma((7,)),
            dma((experts,)),
            dma((chips,)),
            dma((chips,)),
            dma((chips,)),
            dma((parts, chips)),
            dma((parts, chips)),
            dma((2, chips + 1)),
            dma((2, chips + 1)),
            dma((parts,)),
            dma((parts,)),
            dma((2,)),
            dma((2,)),
            dma((experts,)),
            dma((experts,)),
        ],
        compiler_params=pltpu.CompilerParams(
            collective_id=0, has_side_effects=True, vmem_limit_bytes=60 * 1024 * 1024
        ),
    )(
        expert_input,
        expert_gain.reshape(1, -1),
        expert_share,
        mixer_input,
        mixer_gain.reshape(1, -1),
        cosine,
        sine,
        sink_logit.reshape(1, -1),
        query_weight,
        key_weight,
        value_weight,
        output_weight,
        gate_weight[0],
        up_weight[0],
        down_weight[0],
    )


def solution(mesh):
    return jax.shard_map(
        shards,
        mesh=mesh,
        in_specs=(
            P("ep", None),
            P(),
            P(None, "tp"),
            P(None, "tp"),
            P(None, "tp"),
            P(None, "tp"),
            P("tp"),
            P("ep", None),
            P(),
            P("ep", None),
            P("ep", None),
            P("ep", None, "tp"),
            P("ep", None, "tp"),
            P("ep", None, "tp"),
        ),
        out_specs=(P("ep", "tp"), P("ep", "tp")),
        check_vma=False,
    )
```

profile of v0, /device:TPU:0, one launch (start us, length us, event | category | flops | bytes accessed | tf_op | source)
XLA Modules:
  0.0 110.9 jit_solution(10300028031937659614)
XLA Ops:
  0.6 0.7 reduce_max.9
  1.3 0.7 fusion.2
  2.0 0.7 fusion.1
  2.8 0.7 select_reduce_fusion
  3.5 0.7 copy.18.share_ref
  4.2 1.3 %sine_multiply_fusion = (f32[256,128]{1,0:T(8,128)}, f32[256,128]{1,0:T(8,128)}) fusion(f32[128]{0:T(128)S(1)} %get-tuple-element.6, f32[128]{0:T(128)S(1)} %get-tuple-element.7, s32[256]{0:T(256)S(1)} %get-tuple-element.4, s32[256]{0:T(256)S(1)} %get-tuple-element.5, pred[128]{0:T(512)(128)(4,1)S(1)} %fusion.4), kind=kLoop, calls=%fused_computation | loop fusion | flops 131072 | bytes 265344 | tf_op jit(solution)/shard_map/mul | solution.py:488
  5.4 102.2 %shard_map.149 = (bf16[256,512]{1,0:T(8,128)(2,1)}, bf16[128,512]{1,0:T(8,128)(2,1)}) custom-call(bf16[128,2048]{1,0:T(8,128)(2,1)} %x_ref.1, f32[1,2048]{1,0:T(1,128)} %bitcast.9, f32[128,8]{1,0:T(8,128)} %copy.18.share_ref, bf16[256,2048]{1,0:T(8,128)(2,1)} %mixer_ref.1, f32[1,2048]{1,0:T(1,128)} %bitcast.10, f32[256,128]{1,0:T(8,128)} %get-tuple-element.3.cosine_ref, ...), custom_call_target="tpu_custom_call" | custom-call | tf_op jit(solution)/shard_map/pallas_call | solution.py:501
  107.6 1.7 %copy.21 = bf16[256,512]{1,0:T(8,128)(2,1)} copy(bf16[256,512]{1,0:T(8,128)(2,1)} %get-tuple-element.10) | data formatting | bytes 524288
  109.3 1.6 %copy.22 = bf16[128,512]{1,0:T(8,128)(2,1)} copy(bf16[128,512]{1,0:T(8,128)(2,1)} %get-tuple-element.11) | data formatting | bytes 262144
  (3 shorter events, 0.0 us)
where the time goes:
time: 111 us
  Pallas kernels  102 us (92%)
  other arithmetic  4.07 us (4%)
  local copies, waits for them, and re-layouts  3.96 us (4%)
    pallas_call x1, Pallas kernels, shards(): pl.pallas_call(functools.partial(exchange, experts, parts), out_shape=(ja...  102 us
    unnamed x2, local copies, waits for them, and re-layouts  3.24 us

commit v1 on v0

v1 whole, which is shorter than its diff:
```python
import functools

import jax
import jax.numpy as jnp
import numpy as np
from jax import lax
from jax.experimental import pallas as pl
from jax.experimental.pallas import tpu as pltpu
from jax.sharding import PartitionSpec as P

HEAD_DIM = 64
TOP_K = 4
WINDOW = 128
GRID_W = 64


EPSILON = 1e-06
LIMIT = 7.0
SLOPE = 1.702
BASE = 10000.0


def normalize(rows, gain):
    values = rows.astype(jnp.float32)
    scaled = values * lax.rsqrt(jnp.mean(values * values, axis=-1, keepdims=True) + EPSILON)
    return (scaled * gain).astype(jnp.bfloat16)


def rotate(values, cosine, sine):
    width = values.shape[1]
    lanes = cosine.shape[1]
    if width < lanes:
        return rotate(jnp.concatenate([values] * (lanes // width), axis=1), cosine, sine)[:, :width]
    spot = lax.broadcasted_iota(jnp.int32, cosine.shape, 1)
    leading = spot % (HEAD_DIM // 2) < HEAD_DIM // 4
    pieces = []
    for start in range(0, width, lanes):
        piece = values[:, start : start + lanes]
        other = jnp.where(
            leading,
            pltpu.roll(piece, lanes - HEAD_DIM // 4, 1),
            pltpu.roll(piece, HEAD_DIM // 4, 1),
        )
        pieces.append(piece * cosine + other * sine)
    return jnp.concatenate(pieces, axis=1)


def activate(gate, up):
    capped = jnp.minimum(gate, LIMIT)
    bounded = jnp.clip(up, -LIMIT, LIMIT)
    return (capped * jax.nn.sigmoid(SLOPE * capped) * (bounded + 1.0)).astype(jnp.bfloat16)


def remote(src, dst, sent, landed, ep, tp):
    return pltpu.make_async_remote_copy(
        src_ref=src,
        dst_ref=dst,
        send_sem=sent,
        recv_sem=landed,
        device_id=(ep, tp),
        device_id_type=pl.DeviceIdType.MESH,
    )


def exchange(
    n,
    t,
    x_hbm,
    gain_ref,
    logit_ref,
    route_ref,
    mixer_hbm,
    mixer_gain_ref,
    frequency_ref,
    sink_ref,
    wq_hbm,
    wk_hbm,
    wv_hbm,
    wo_hbm,
    wg_hbm,
    wu_hbm,
    wd_hbm,
    mixer_out,
    expert_out,
    x_ref,
    mixer_ref,
    tokens,
    hidden,
    heads,
    shares,
    half_out,
    half_in,
    result,
    returned,
    kept_half,
    queries,
    around,
    wq,
    wk,
    wv,
    wo,
    wg,
    wu,
    wd,
    local_sem,
    token_recv,
    up_send,
    down_send,
    core_send,
    hidden_send,
    hidden_recv,
    pass_send,
    head_send,
    head_recv,
    head_pass_send,
    edge_send,
    edge_recv,
    share_send,
    share_recv,
    half_send,
    half_recv,
    result_send,
    result_recv,
):
    ep, tp = lax.axis_index("ep"), lax.axis_index("tp")
    chips = n // 2
    z, core = ep // 2, ep % 2
    partner = 2 * z + 1 - core
    rows = x_ref.shape[0]
    pair = 2 * rows
    part = wg.shape[1]
    length = mixer_ref.shape[0]
    kept = wk.shape[1]
    spread = wq.shape[1]
    square = t == 4
    direct = (1, 2) if square else tuple(range(1, t))

    def peer(k):
        if not square:
            return lax.rem(tp + k, t)
        return lax.rem(tp + (k // 2) * 2 + (k % 2) * (1 - 2 * (tp % 2)) + t, t)

    def block(index, size):
        return pl.ds(pl.multiple_of(index * size, size), size)

    loads = [
        pltpu.make_async_copy(a, b, local_sem.at[i])
        for i, (a, b) in enumerate((
            (x_hbm, x_ref),
            (wg_hbm, wg),
            (wu_hbm, wu),
            (mixer_hbm, mixer_ref),
            (wk_hbm, wk),
            (wv_hbm, wv),
            (wq_hbm, wq),
            (wd_hbm, wd),
            (wo_hbm, wo),
        ))
    ]
    for load in loads:
        load.start()

    barrier = pltpu.get_barrier_semaphore()
    for k in range(1, n):
        pl.semaphore_signal(
            barrier,
            inc=1,
            device_id=(lax.rem(ep + k, n), tp),
            device_id_type=pl.DeviceIdType.MESH,
        )
    for k in range(1, t):
        pl.semaphore_signal(
            barrier,
            inc=1,
            device_id=(ep, peer(k)),
            device_id_type=pl.DeviceIdType.MESH,
        )

    logits = logit_ref[...]
    raised = jnp.exp(logits - jnp.max(logits, axis=0, keepdims=True))
    chances = raised / jnp.sum(raised, axis=0, keepdims=True)
    number = lax.broadcasted_iota(jnp.int32, (n, rows), 0)
    share = jnp.zeros((n, rows), jnp.float32)
    for k in range(TOP_K):
        share += jnp.where(route_ref[k : k + 1, :] == number, chances[k : k + 1, :], 0.0)
    shares[ep] = share

    loads[0].wait()
    tokens[block(ep, rows), :] = normalize(x_ref[...], gain_ref[...])
    pl.semaphore_wait(barrier, n + t - 2)

    def token_copy(slot, sent, target):
        piece = tokens.at[block(slot, rows)]
        return remote(piece, piece, sent, token_recv.at[slot], target, tp)

    def up_copy(place):
        return token_copy(2 * place + core, up_send.at[place], ep + 2)

    def down_copy(place):
        return token_copy(2 * place + core, down_send.at[place], ep - 2)

    def core_copy(place):
        return token_copy(2 * place + core, core_send.at[place], partner)

    def token_wait(slot):
        token_copy(slot, core_send.at[0], partner).wait_recv()

    def share_copy(k):
        piece = shares.at[ep]
        target = lax.rem(ep + k, n)
        return remote(piece, piece, share_send.at[k], share_recv.at[ep], target, tp)

    def share_wait(slot):
        piece = shares.at[slot]
        remote(piece, piece, share_send.at[0], share_recv.at[slot], partner, tp).wait_recv()

    lowest, highest = z == 0, z == chips - 1

    @pl.when(jnp.logical_not(highest))
    def _():
        up_copy(z).start()

    @pl.when(jnp.logical_not(lowest))
    def _():
        down_copy(z).start()

    core_copy(z).start()
    for k in range(1, n):
        share_copy(k).start()

    def hidden_piece(source, place, half):
        return hidden.at[
            block(2 * place + half, rows), pl.ds(pl.multiple_of(source * part, part), part)
        ]

    def hidden_copy(source, place, half, k):
        piece = hidden_piece(source, place, half)
        return remote(
            piece,
            piece,
            hidden_send.at[k, place, half],
            hidden_recv.at[source, place, half],
            ep,
            peer(k),
        )

    def hidden_forward(place, way):
        source = peer(2 - way)
        piece = hidden_piece(source, place, 1 - way)
        return remote(
            piece,
            piece,
            pass_send.at[way, place],
            hidden_recv.at[source, place, 1 - way],
            ep,
            peer(1 + way),
        )

    def hidden_pass(place):
        if square:
            for way in range(2):
                hidden_copy(peer(2 - way), place, 1 - way, 2 - way).wait_recv()
                hidden_forward(place, way).start()

    def hidden_wait(place):
        for k in range(1, t):
            for half in range(2):
                if not (square and (k, half) in ((1, 0), (2, 1))):
                    hidden_copy(peer(k), place, half, direct[0]).wait_recv()

    def head_piece(source, half):
        return heads.at[
            pl.ds(half * (length // 2), length // 2),
            pl.ds(pl.multiple_of(source * spread, spread), spread),
        ]

    def head_copy(source, half, k):
        piece = head_piece(source, half)
        return remote(
            piece, piece, head_send.at[k, half], head_recv.at[source, half], ep, peer(k)
        )

    def head_forward(way):
        source = peer(2 - way)
        piece = head_piece(source, 1 - way)
        return remote(
            piece,
            piece,
            head_pass_send.at[way],
            head_recv.at[source, 1 - way],
            ep,
            peer(1 + way),
        )

    def head_pass():
        if square:
            for way in range(2):
                head_copy(peer(2 - way), 1 - way, 2 - way).wait_recv()
                head_forward(way).start()

    def head_wait():
        for k in range(1, t):
            for half in range(2):
                if not (square and (k, half) in ((1, 0), (2, 1))):
                    head_copy(peer(k), half, direct[0]).wait_recv()

    def first_half(place):
        token_wait(2 * place + 1 - core)
        inside = block(place, pair)
        span = min(256, part)
        for start in range(0, part, span):
            cut = slice(start, start + span)
            gate = jnp.dot(tokens[inside, :], wg[:, cut], preferred_element_type=jnp.float32)
            up = jnp.dot(tokens[inside, :], wu[:, cut], preferred_element_type=jnp.float32)
            column = pl.ds(pl.multiple_of(tp * part + start, span), span)
            hidden[inside, column] = activate(gate, up)
        for order in range(2):
            for k in direct:
                hidden_copy(tp, place, order if k != 2 else 1 - order, k).start()

    loads[1].wait()
    loads[2].wait()
    first_half(z)

    loads[3].wait()
    normed = normalize(mixer_ref[...], mixer_gain_ref[...])
    lanes = 2 * HEAD_DIM
    spot = lax.broadcasted_iota(jnp.int32, (length, lanes), 1)
    token = ep * length + lax.broadcasted_iota(jnp.int32, (length, lanes), 0)
    turn = jnp.where(spot % HEAD_DIM < HEAD_DIM // 2, token // GRID_W, token % GRID_W)
    turn = turn.astype(jnp.float32) * frequency_ref[...]
    cosine = jnp.cos(turn)
    sine = jnp.sin(turn) * jnp.where(spot % (HEAD_DIM // 2) < HEAD_DIM // 4, -1.0, 1.0)
    own = slice(WINDOW, WINDOW + length)
    for load in loads[4:6]:
        load.wait()
    keys = jnp.dot(normed, wk[...], preferred_element_type=jnp.float32)
    around[own, 0:kept] = rotate(keys, cosine, sine).astype(jnp.bfloat16)
    around[own, kept:] = jnp.dot(normed, wv[...], preferred_element_type=jnp.float32).astype(
        jnp.bfloat16
    )

    def edge_copy(way):
        source, target = (length, 0) if way == 0 else (WINDOW, WINDOW + length)
        return remote(
            around.at[pl.ds(source, WINDOW)],
            around.at[pl.ds(target, WINDOW)],
            edge_send.at[way],
            edge_recv.at[way],
            ep + (1 if way == 0 else -1),
            tp,
        )

    first, last = ep == 0, ep == n - 1

    @pl.when(jnp.logical_not(last))
    def _():
        edge_copy(0).start()

    @pl.when(jnp.logical_not(first))
    def _():
        edge_copy(1).start()

    @pl.when(first)
    def _():
        around[0:WINDOW, :] = jnp.zeros((WINDOW, around.shape[1]), jnp.bfloat16)

    @pl.when(last)
    def _():
        around[WINDOW + length :, :] = jnp.zeros((WINDOW, around.shape[1]), jnp.bfloat16)

    loads[6].wait()
    turned = jnp.dot(normed, wq[...], preferred_element_type=jnp.float32)
    queries[...] = rotate(turned, cosine, sine).astype(jnp.bfloat16)

    def attend(number, carry):
        inside = pl.ds(pl.multiple_of(number * WINDOW, WINDOW), WINDOW)
        seen = pl.ds(pl.multiple_of(number * WINDOW, WINDOW), 3 * WINDOW)
        shape = (WINDOW, 3 * WINDOW)
        line = lax.broadcasted_iota(jnp.int32, shape, 0)
        key = lax.broadcasted_iota(jnp.int32, shape, 1)
        place = ep * length + (number - 1) * WINDOW + key
        allowed = (key >= line) & (key <= line + 2 * WINDOW) & (place >= 0) & (place < n * length)
        group = queries.shape[1] // kept
        allowed = jnp.concatenate([allowed] * group, axis=0)
        for head in range(kept // HEAD_DIM):
            first = head * group
            query = jnp.concatenate(
                [
                    queries[inside, (first + r) * HEAD_DIM : (first + r + 1) * HEAD_DIM]
                    for r in range(group)
                ],
                axis=0,
            )
            sinks = jnp.concatenate(
                [
                    jnp.broadcast_to(sink_ref[:, first + r : first + r + 1], (WINDOW, 1))
                    for r in range(group)
                ],
                axis=0,
            )
            near_keys = around[seen, head * HEAD_DIM : (head + 1) * HEAD_DIM]
            near_values = around[seen, kept + head * HEAD_DIM : kept + (head + 1) * HEAD_DIM]
            scores = lax.dot_general(
                query,
                near_keys,
                (((1,), (1,)), ((), ())),
                preferred_element_type=jnp.float32,
            ) * HEAD_DIM ** (-0.5)
            scores = jnp.where(allowed, scores, -1e30)
            top = jnp.maximum(jnp.max(scores, axis=-1, keepdims=True), sinks)
            weights = jnp.exp(scores - top)
            denominator = jnp.sum(weights, axis=-1, keepdims=True) + jnp.exp(sinks - top)
            share = (weights * (1.0 / denominator)).astype(jnp.bfloat16)
            mixed = jnp.dot(share, near_values, preferred_element_type=jnp.float32)
            mixed = mixed.astype(jnp.bfloat16)
            width = group * HEAD_DIM
            column = pl.ds(pl.multiple_of(tp * spread + first * HEAD_DIM, width), width)
            heads[inside, column] = jnp.concatenate(
                [mixed[r * WINDOW : (r + 1) * WINDOW] for r in range(group)], axis=1
            )
        return carry

    def attention():
        @pl.when(jnp.logical_not(first))
        def _():
            edge_copy(0).wait_recv()

        @pl.when(jnp.logical_not(last))
        def _():
            edge_copy(1).wait_recv()

        lax.fori_loop(0, length // WINDOW, attend, 0)
        for order in range(2):
            for k in direct:
                head_copy(tp, order if k != 2 else 1 - order, k).start()

    def half_copy(place):
        return remote(
            half_out.at[place],
            half_in.at[place],
            half_send.at[place],
            half_recv.at[place],
            partner,
            tp,
        )

    def result_copy(place, source):
        return remote(
            result.at[place],
            returned.at[source],
            result_send.at[place],
            result_recv.at[source],
            2 * place + core,
            tp,
        )

    def scaled(slot):
        total = jnp.dot(hidden[block(slot, rows), :], wd[...], preferred_element_type=jnp.float32)
        line = shares[slot, pl.ds(ep, 1), :]
        column = jnp.transpose(jnp.broadcast_to(line, (rows, rows)))
        return jnp.concatenate(
            [total[:, i : i + rows] * column for i in range(0, total.shape[1], rows)], axis=1
        )

    def second_half(place, mine):
        hidden_wait(place)
        for side in (1 - core, core):
            slot = 2 * place + side
            if mine:
                @pl.when(slot != ep)
                def _():
                    share_wait(slot)
            else:
                share_wait(slot)
        half_out[place] = scaled(2 * place + 1 - core).astype(jnp.bfloat16)
        half_copy(place).start()
        kept_half[...] = scaled(2 * place + core)
        half_copy(place).wait_recv()
        total = kept_half[...] + half_in[place].astype(jnp.float32)
        if mine:
            returned[place] = total.astype(jnp.bfloat16)
        else:
            result[place] = total.astype(jnp.bfloat16)
            result_copy(place, z).start()

    def sides(hop, action):
        def side(k, carry):
            place = z + (2 * k - 1) * hop

            @pl.when((place >= 0) & (place < chips))
            def _():
                action(place, k)

            return carry

        lax.fori_loop(0, 2, side, 0)

    def arrive(hop):
        below, above = z - hop, z + hop

        @pl.when(below >= 0)
        def _():
            token_wait(2 * below + core)

            @pl.when(jnp.logical_not(highest))
            def _():
                up_copy(below).start()

            core_copy(below).start()

        @pl.when(above < chips)
        def _():
            token_wait(2 * above + core)

            @pl.when(jnp.logical_not(lowest))
            def _():
                down_copy(above).start()

            core_copy(above).start()

    def pass_one(hop):
        below, above = z - hop, z + hop

        @pl.when((below >= 0) | (above < chips))
        def _():
            hidden_pass(jnp.where(below >= 0, below, above))

    def pass_two(hop):
        below, above = z - hop, z + hop

        @pl.when((below >= 0) & (above < chips))
        def _():
            hidden_pass(above)

    hidden_pass(z)
    arrive(1)
    sides(1, lambda place, k: first_half(place))
    attention()
    loads[7].wait()
    second_half(z, True)
    pass_one(1)

    def hop_step(hop, carry):
        arrive(hop)
        pass_two(hop - 1)
        sides(hop, lambda place, k: first_half(place))

        @pl.when(hop == 2)
        def _():
            head_pass()

        sides(hop - 1, lambda place, k: second_half(place, False))
        pass_one(hop)
        return carry

    lax.fori_loop(2, chips, hop_step, 0)
    pass_two(chips - 1)
    sides(chips - 1, lambda place, k: second_half(place, False))
    loads[8].wait()
    head_wait()
    mixer_out[...] = jnp.dot(heads[...], wo[...], preferred_element_type=jnp.float32).astype(
        jnp.bfloat16
    )

    for k in range(1, chips):
        source = lax.rem(z + k, chips)
        result_copy(source, source).wait_recv()
    total = returned[0].astype(jnp.float32)
    for source in range(1, chips):
        total += returned[source].astype(jnp.float32)
    expert_out[...] = total.astype(jnp.bfloat16)

    for place in range(chips):
        @pl.when((place <= z) & jnp.logical_not(highest))
        def _():
            up_copy(place).wait_send()

        @pl.when((place >= z) & jnp.logical_not(lowest))
        def _():
            down_copy(place).wait_send()

        core_copy(place).wait_send()
        half_copy(place).wait_send()
        for k in direct:
            for half in range(2):
                hidden_copy(tp, place, half, k).wait_send()
        if square:
            for way in range(2):
                hidden_forward(place, way).wait_send()

        @pl.when(place != z)
        def _():
            result_copy(place, z).wait_send()

    for k in direct:
        for half in range(2):
            head_copy(tp, half, k).wait_send()
    if square:
        for way in range(2):
            head_forward(way).wait_send()

    @pl.when(jnp.logical_not(last))
    def _():
        edge_copy(0).wait_send()

    @pl.when(jnp.logical_not(first))
    def _():
        edge_copy(1).wait_send()

    for k in range(1, n):
        share_copy(k).wait_send()


def shards(
    mixer_input,
    mixer_gain,
    query_weight,
    key_weight,
    value_weight,
    output_weight,
    sink_logit,
    expert_input,
    expert_gain,
    routes,
    route_logits,
    gate_weight,
    up_weight,
    down_weight,
):
    tokens = mixer_input.shape[0]
    lanes = 2 * HEAD_DIM
    quarter = HEAD_DIM // 4
    spot = np.arange(lanes) % quarter
    frequency = (BASE ** (-spot.astype(np.float32) / np.float32(quarter))).astype(np.float32)[None]
    experts = lax.axis_size("ep")
    parts = lax.axis_size("tp")
    rows, width = expert_input.shape
    part = gate_weight.shape[2]
    vmem = pl.BlockSpec(memory_space=pltpu.VMEM)
    anywhere = pl.BlockSpec(memory_space=pl.ANY)
    chips = experts // 2
    dma = pltpu.SemaphoreType.DMA
    columns = down_weight.shape[2]
    spread = query_weight.shape[1]
    half = jnp.bfloat16
    return pl.pallas_call(
        functools.partial(exchange, experts, parts),
        out_shape=(
            jax.ShapeDtypeStruct((tokens, output_weight.shape[1]), half),
            jax.ShapeDtypeStruct((rows, columns), half),
        ),
        in_specs=[anywhere, vmem, vmem, vmem, anywhere, vmem, vmem, vmem] + [anywhere] * 7,
        out_specs=(vmem, vmem),
        scratch_shapes=[
            pltpu.VMEM((rows, width), half),
            pltpu.VMEM(mixer_input.shape, half),
            pltpu.VMEM((experts * rows, width), half),
            pltpu.VMEM((experts * rows, parts * part), half),
            pltpu.VMEM((tokens, parts * spread), half),
            pltpu.VMEM((experts, experts, rows), jnp.float32),
            pltpu.VMEM((chips, rows, columns), half),
            pltpu.VMEM((chips, rows, columns), half),
            pltpu.VMEM((chips, rows, columns), half),
            pltpu.VMEM((chips, rows, columns), half),
            pltpu.VMEM((rows, columns), jnp.float32),
            pltpu.VMEM((tokens, spread), half),
            pltpu.VMEM((tokens + 2 * WINDOW, 2 * key_weight.shape[1]), half),
            pltpu.VMEM(query_weight.shape, half),
            pltpu.VMEM(key_weight.shape, half),
            pltpu.VMEM(value_weight.shape, half),
            pltpu.VMEM(output_weight.shape, half),
            pltpu.VMEM(gate_weight.shape[1:], half),
            pltpu.VMEM(up_weight.shape[1:], half),
            pltpu.VMEM(down_weight.shape[1:], half),
            dma((9,)),
            dma((experts,)),
            dma((chips,)),
            dma((chips,)),
            dma((chips,)),
            dma((parts, chips, 2)),
            dma((parts, chips, 2)),
            dma((2, chips)),
            dma((parts, 2)),
            dma((parts, 2)),
            dma((2,)),
            dma((2,)),
            dma((2,)),
            dma((experts,)),
            dma((experts,)),
            dma((chips,)),
            dma((chips,)),
            dma((chips,)),
            dma((chips,)),
        ],
        compiler_params=pltpu.CompilerParams(
            collective_id=0, has_side_effects=True, vmem_limit_bytes=60 * 1024 * 1024
        ),
    )(
        expert_input,
        expert_gain.reshape(1, -1),
        route_logits.T,
        routes.T,
        mixer_input,
        mixer_gain.reshape(1, -1),
        jnp.asarray(frequency),
        sink_logit.reshape(1, -1),
        query_weight,
        key_weight,
        value_weight,
        output_weight,
        gate_weight[0],
        up_weight[0],
        down_weight[0],
    )


def solution(mesh):
    return jax.shard_map(
        shards,
        mesh=mesh,
        in_specs=(
            P("ep", None),
            P(),
            P(None, "tp"),
            P(None, "tp"),
            P(None, "tp"),
            P(None, "tp"),
            P("tp"),
            P("ep", None),
            P(),
            P("ep", None),
            P("ep", None),
            P("ep", None, "tp"),
            P("ep", None, "tp"),
            P("ep", None, "tp"),
        ),
        out_specs=(P("ep", "tp"), P("ep", "tp")),
        check_vma=False,
    )
```

time: 111 us -> 72.8 us (0.66)
  Pallas kernels: 102 us -> 68.7 us
  other arithmetic: 4.07 us -> 0 us
    pallas_call x1, Pallas kernels: 102 us -> 68.7 us  [shards(): pl.pallas_call(functools.partial(exchange, experts, parts), out_shape=(ja...]
    reduce_sum x2 -> x0, other arithmetic: 1.39 us -> none  [the longest x1 0.7 us: shards(): chances = jax.nn.softmax(route_logits, axis=-1)]
    mul x1 -> x0, other arithmetic: 1.26 us -> none  [shards(): jnp.sin(turn) * jnp.where(spot % (HEAD_DIM // 2) < quarter, -1.0, 1.0)]
where the time goes in v1:
time: 72.8 us; the launch traced here: 72.6 us
  Pallas kernels  68.7 us (94%)
  local copies, waits for them, and re-layouts  3.24 us (4%)
    pallas_call x1, Pallas kernels, shards(): pl.pallas_call(functools.partial(exchange, experts, parts), out_shape=(ja...  68.7 us
    unnamed x2, local copies, waits for them, and re-layouts  3.24 us

profile of v1, /device:TPU:0, one launch (start us, length us, event | category | flops | bytes accessed | tf_op | source)
XLA Modules:
  0.0 72.6 jit_solution(11324938773553027916)
XLA Ops:
  0.6 68.7 %shard_map.158 = (bf16[256,512]{1,0:T(8,128)(2,1)}, bf16[128,512]{1,0:T(8,128)(2,1)}) custom-call(bf16[128,2048]{1,0:T(8,128)(2,1)} %x_hbm.1, f32[1,2048]{1,0:T(1,128)} %bitcast.11, f32[4,128]{1,0:T(4,128)} %bitcast.13, s32[4,128]{1,0:T(4,128)} %bitcast.14, bf16[256,2048]{1,0:T(8,128)(2,1)} %mixer_hbm.1, f32[1,2048]{1,0:T(1,128)} %bitcast.12, ...), custom_call_target="tpu_custom_call" | custom-call | tf_op jit(solution)/shard_map/pallas_call | solution.py:647
  69.4 1.7 %copy.19 = bf16[256,512]{1,0:T(8,128)(2,1)} copy(bf16[256,512]{1,0:T(8,128)(2,1)} %get-tuple-element.4) | data formatting | bytes 524288
  71.0 1.6 %copy.20 = bf16[128,512]{1,0:T(8,128)(2,1)} copy(bf16[128,512]{1,0:T(8,128)(2,1)} %get-tuple-element.5) | data formatting | bytes 262144

commit v2 on v1

--- a/solution.py
+++ b/solution.py
@@ -12,6 +12,9 @@
 TOP_K = 4
 WINDOW = 128
 GRID_W = 64
+SPLIT = 2
+EARLY = 0
+LATE = 3
 
 
 EPSILON = 1e-06
@@ -93,6 +96,9 @@
     result,
     returned,
     kept_half,
+    scales,
+    cosine_ref,
+    sine_ref,
     queries,
     around,
     wq,
@@ -127,7 +133,8 @@
     z, core = ep // 2, ep % 2
     partner = 2 * z + 1 - core
     rows = x_ref.shape[0]
-    pair = 2 * rows
+    size = rows // SPLIT
+    pair = 2 * size
     part = wg.shape[1]
     length = mixer_ref.shape[0]
     kept = wk.shape[1]
@@ -185,22 +192,38 @@
         share += jnp.where(route_ref[k : k + 1, :] == number, chances[k : k + 1, :], 0.0)
     shares[ep] = share
 
+    lanes = 2 * HEAD_DIM
+    spot = lax.broadcasted_iota(jnp.int32, (length, lanes), 1)
+    token = ep * length + lax.broadcasted_iota(jnp.int32, (length, lanes), 0)
+    turn = jnp.where(spot % HEAD_DIM < HEAD_DIM // 2, token // GRID_W, token % GRID_W)
+    turn = turn.astype(jnp.float32) * frequency_ref[...]
+    cosine_ref[...] = jnp.cos(turn)
+    sine_ref[...] = jnp.sin(turn) * jnp.where(spot % (HEAD_DIM // 2) < HEAD_DIM // 4, -1.0, 1.0)
+
     loads[0].wait()
-    tokens[block(ep, rows), :] = normalize(x_ref[...], gain_ref[...])
-    pl.semaphore_wait(barrier, n + t - 2)
+    fresh = normalize(x_ref[...], gain_ref[...])
+    for sub in range(SPLIT):
+        inside = block(2 * (z * SPLIT + sub) + core, size)
+        tokens[inside, :] = fresh[sub * size : (sub + 1) * size]
+
+    def unit(place, sub):
+        return place * SPLIT + sub
 
     def token_copy(slot, sent, target):
-        piece = tokens.at[block(slot, rows)]
+        piece = tokens.at[block(slot, size)]
         return remote(piece, piece, sent, token_recv.at[slot], target, tp)
 
-    def up_copy(place):
-        return token_copy(2 * place + core, up_send.at[place], ep + 2)
-
-    def down_copy(place):
-        return token_copy(2 * place + core, down_send.at[place], ep - 2)
-
-    def core_copy(place):
-        return token_copy(2 * place + core, core_send.at[place], partner)
+    def up_copy(place, sub):
+        u = unit(place, sub)
+        return token_copy(2 * u + core, up_send.at[u], ep + 2)
+
+    def down_copy(place, sub):
+        u = unit(place, sub)
+        return token_copy(2 * u + core, down_send.at[u], ep - 2)
+
+    def core_copy(place, sub):
+        u = unit(place, sub)
+        return token_copy(2 * u + core, core_send.at[u], partner)
 
     def token_wait(slot):
         token_copy(slot, core_send.at[0], partner).wait_recv()
@@ -216,61 +239,58 @@
 
     lowest, highest = z == 0, z == chips - 1
 
-    @pl.when(jnp.logical_not(highest))
-    def _():
-        up_copy(z).start()
-
-    @pl.when(jnp.logical_not(lowest))
-    def _():
-        down_copy(z).start()
-
-    core_copy(z).start()
-    for k in range(1, n):
-        share_copy(k).start()
-
-    def hidden_piece(source, place, half):
+    def spread_own(sub):
+        @pl.when(jnp.logical_not(highest))
+        def _():
+            up_copy(z, sub).start()
+
+        @pl.when(jnp.logical_not(lowest))
+        def _():
+            down_copy(z, sub).start()
+
+    def hidden_piece(source, u, half):
         return hidden.at[
-            block(2 * place + half, rows), pl.ds(pl.multiple_of(source * part, part), part)
+            block(2 * u + half, size), pl.ds(pl.multiple_of(source * part, part), part)
         ]
 
-    def hidden_copy(source, place, half, k):
-        piece = hidden_piece(source, place, half)
+    def hidden_copy(source, u, half, k):
+        piece = hidden_piece(source, u, half)
         return remote(
             piece,
             piece,
-            hidden_send.at[k, place, half],
-            hidden_recv.at[source, place, half],
+            hidden_send.at[k, u, half],
+            hidden_recv.at[source, u, half],
             ep,
             peer(k),
         )
 
-    def hidden_forward(place, way):
+    def hidden_forward(u, way):
         source = peer(2 - way)
-        piece = hidden_piece(source, place, 1 - way)
+        piece = hidden_piece(source, u, 1 - way)
         return remote(
             piece,
             piece,
-            pass_send.at[way, place],
-            hidden_recv.at[source, place, 1 - way],
+            pass_send.at[way, u],
+            hidden_recv.at[source, u, 1 - way],
             ep,
             peer(1 + way),
         )
 
-    def hidden_pass(place):
+    def hidden_pass(u):
         if square:
             for way in range(2):
-                hidden_copy(peer(2 - way), place, 1 - way, 2 - way).wait_recv()
-                hidden_forward(place, way).start()
-
-    def hidden_wait(place):
+                hidden_copy(peer(2 - way), u, 1 - way, 2 - way).wait_recv()
+                hidden_forward(u, way).start()
+
+    def hidden_wait(u):
         for k in range(1, t):
             for half in range(2):
                 if not (square and (k, half) in ((1, 0), (2, 1))):
-                    hidden_copy(peer(k), place, half, direct[0]).wait_recv()
+                    hidden_copy(peer(k), u, half, direct[0]).wait_recv()
 
     def head_piece(source, half):
         return heads.at[
-            pl.ds(half * (length // 2), length // 2),
+            block(half, length // 2),
             pl.ds(pl.multiple_of(source * spread, spread), spread),
         ]
 
@@ -304,36 +324,50 @@
                 if not (square and (k, half) in ((1, 0), (2, 1))):
                     head_copy(peer(k), half, direct[0]).wait_recv()
 
-    def first_half(place):
-        token_wait(2 * place + 1 - core)
-        inside = block(place, pair)
+    def expand(slots):
         span = min(256, part)
         for start in range(0, part, span):
             cut = slice(start, start + span)
-            gate = jnp.dot(tokens[inside, :], wg[:, cut], preferred_element_type=jnp.float32)
-            up = jnp.dot(tokens[inside, :], wu[:, cut], preferred_element_type=jnp.float32)
+            lines = jnp.concatenate([tokens[block(slot, size), :] for slot in slots], axis=0)
+            gate = jnp.dot(lines, wg[:, cut], preferred_element_type=jnp.float32)
+            up = jnp.dot(lines, wu[:, cut], preferred_element_type=jnp.float32)
             column = pl.ds(pl.multiple_of(tp * part + start, span), span)
-            hidden[inside, column] = activate(gate, up)
+            active = activate(gate, up)
+            for i, slot in enumerate(slots):
+                hidden[block(slot, size), column] = active[i * size : (i + 1) * size]
+
+    def first_half(u):
+        token_wait(2 * u + 1 - core)
+        expand([2 * u, 2 * u + 1])
         for order in range(2):
             for k in direct:
-                hidden_copy(tp, place, order if k != 2 else 1 - order, k).start()
+                hidden_copy(tp, u, order if k != 2 else 1 - order, k).start()
+
+    def first_own(side):
+        expand([2 * unit(z, sub) + side for sub in range(SPLIT)])
+
+    def send_own(side):
+        for sub in range(SPLIT):
+            for k in direct:
+                hidden_copy(tp, unit(z, sub), side, k).start()
 
     loads[1].wait()
     loads[2].wait()
-    first_half(z)
+    first_own(core)
+    pl.semaphore_wait(barrier, n + t - 2)
+    for k in range(1, n):
+        share_copy(k).start()
+    spread_own(0)
+    for sub in range(SPLIT):
+        core_copy(z, sub).start()
+    send_own(core)
 
     loads[3].wait()
     normed = normalize(mixer_ref[...], mixer_gain_ref[...])
-    lanes = 2 * HEAD_DIM
-    spot = lax.broadcasted_iota(jnp.int32, (length, lanes), 1)
-    token = ep * length + lax.broadcasted_iota(jnp.int32, (length, lanes), 0)
-    turn = jnp.where(spot % HEAD_DIM < HEAD_DIM // 2, token // GRID_W, token % GRID_W)
-    turn = turn.astype(jnp.float32) * frequency_ref[...]
-    cosine = jnp.cos(turn)
-    sine = jnp.sin(turn) * jnp.where(spot % (HEAD_DIM // 2) < HEAD_DIM // 4, -1.0, 1.0)
     own = slice(WINDOW, WINDOW + length)
     for load in loads[4:6]:
         load.wait()
+    cosine, sine = cosine_ref[...], sine_ref[...]
     keys = jnp.dot(normed, wk[...], preferred_element_type=jnp.float32)
     around[own, 0:kept] = rotate(keys, cosine, sine).astype(jnp.bfloat16)
     around[own, kept:] = jnp.dot(normed, wv[...], preferred_element_type=jnp.float32).astype(
@@ -361,6 +395,9 @@
     def _():
         edge_copy(1).start()
 
+    for sub in range(1, SPLIT):
+        spread_own(sub)
+
     @pl.when(first)
     def _():
         around[0:WINDOW, :] = jnp.zeros((WINDOW, around.shape[1]), jnp.bfloat16)
@@ -368,6 +405,11 @@
     @pl.when(last)
     def _():
         around[WINDOW + length :, :] = jnp.zeros((WINDOW, around.shape[1]), jnp.bfloat16)
+
+    for sub in range(SPLIT):
+        token_wait(2 * unit(z, sub) + 1 - core)
+    first_own(1 - core)
+    send_own(1 - core)
 
     loads[6].wait()
     turned = jnp.dot(normed, wq[...], preferred_element_type=jnp.float32)
@@ -421,68 +463,65 @@
             )
         return carry
 
-    def attention():
-        @pl.when(jnp.logical_not(first))
+    def attention(half):
+        @pl.when((half == 0) & jnp.logical_not(first))
         def _():
             edge_copy(0).wait_recv()
 
-        @pl.when(jnp.logical_not(last))
+        @pl.when((half == 1) & jnp.logical_not(last))
         def _():
             edge_copy(1).wait_recv()
 
-        lax.fori_loop(0, length // WINDOW, attend, 0)
-        for order in range(2):
-            for k in direct:
-                head_copy(tp, order if k != 2 else 1 - order, k).start()
-
-    def half_copy(place):
+        count = length // 2 // WINDOW
+        lax.fori_loop(half * count, (half + 1) * count, attend, 0)
+        for k in direct:
+            head_copy(tp, half, k).start()
+
+    def half_copy(u):
         return remote(
-            half_out.at[place],
-            half_in.at[place],
-            half_send.at[place],
-            half_recv.at[place],
-            partner,
+            half_out.at[u], half_in.at[u], half_send.at[u], half_recv.at[u], partner, tp
+        )
+
+    def result_copy(u, source):
+        return remote(
+            result.at[u],
+            returned.at[source, u % SPLIT],
+            result_send.at[u],
+            result_recv.at[source, u % SPLIT],
+            2 * (u // SPLIT) + core,
             tp,
         )
 
-    def result_copy(place, source):
-        return remote(
-            result.at[place],
-            returned.at[source],
-            result_send.at[place],
-            result_recv.at[source],
-            2 * place + core,
-            tp,
-        )
-
-    def scaled(slot):
-        total = jnp.dot(hidden[block(slot, rows), :], wd[...], preferred_element_type=jnp.float32)
+    def spread_shares(slot, carry):
+        @pl.when(slot != ep)
+        def _():
+            share_wait(slot)
+
         line = shares[slot, pl.ds(ep, 1), :]
         column = jnp.transpose(jnp.broadcast_to(line, (rows, rows)))
+        for sub in range(SPLIT):
+            inside = block(2 * unit(slot // 2, sub) + slot % 2, size)
+            scales[inside, :] = column[sub * size : (sub + 1) * size]
+        return carry
+
+    def scaled(slot):
+        inside = block(slot, size)
+        total = jnp.dot(hidden[inside, :], wd[...], preferred_element_type=jnp.float32)
+        column = scales[inside, :]
         return jnp.concatenate(
             [total[:, i : i + rows] * column for i in range(0, total.shape[1], rows)], axis=1
         )
 
-    def second_half(place, mine):
-        hidden_wait(place)
-        for side in (1 - core, core):
-            slot = 2 * place + side
-            if mine:
-                @pl.when(slot != ep)
-                def _():
-                    share_wait(slot)
-            else:
-                share_wait(slot)
-        half_out[place] = scaled(2 * place + 1 - core).astype(jnp.bfloat16)
-        half_copy(place).start()
-        kept_half[...] = scaled(2 * place + core)
-        half_copy(place).wait_recv()
-        total = kept_half[...] + half_in[place].astype(jnp.float32)
-        if mine:
-            returned[place] = total.astype(jnp.bfloat16)
-        else:
-            result[place] = total.astype(jnp.bfloat16)
-            result_copy(place, z).start()
+    def second_half(u):
+        hidden_wait(u)
+        half_out[u] = scaled(2 * u + 1 - core).astype(jnp.bfloat16)
+        half_copy(u).start()
+        kept_half[u] = scaled(2 * u + core)
+
+    def combine(u):
+        half_copy(u).wait_recv()
+        total = kept_half[u] + half_in[u].astype(jnp.float32)
+        result[u] = total.astype(jnp.bfloat16)
 
     def sides(hop, action):
         def side(k, carry):
@@ -496,102 +535,181 @@
 
         lax.fori_loop(0, 2, side, 0)
 
-    def arrive(hop):
+    def arrive(hop, sub):
         below, above = z - hop, z + hop
 
         @pl.when(below >= 0)
         def _():
-            token_wait(2 * below + core)
+            token_wait(2 * unit(below, sub) + core)
 
             @pl.when(jnp.logical_not(highest))
             def _():
-                up_copy(below).start()
-
-            core_copy(below).start()
+                up_copy(below, sub).start()
+
+            core_copy(below, sub).start()
 
         @pl.when(above < chips)
         def _():
-            token_wait(2 * above + core)
+            token_wait(2 * unit(above, sub) + core)
 
             @pl.when(jnp.logical_not(lowest))
             def _():
-                down_copy(above).start()
-
-            core_copy(above).start()
-
-    def pass_one(hop):
+                down_copy(above, sub).start()
+
+            core_copy(above, sub).start()
+
+    steps = (chips - 1) * SPLIT
+
+    def one(index, action):
+        hop, sub = 1 + index // SPLIT, index % SPLIT
         below, above = z - hop, z + hop
 
         @pl.when((below >= 0) | (above < chips))
         def _():
-            hidden_pass(jnp.where(below >= 0, below, above))
-
-    def pass_two(hop):
+            action(unit(jnp.where(below >= 0, below, above), sub))
+
+    def two(index, action):
+        hop, sub = 1 + index // SPLIT, index % SPLIT
         below, above = z - hop, z + hop
 
         @pl.when((below >= 0) & (above < chips))
         def _():
-            hidden_pass(above)
-
-    hidden_pass(z)
-    arrive(1)
-    sides(1, lambda place, k: first_half(place))
-    attention()
-    loads[7].wait()
-    second_half(z, True)
-    pass_one(1)
-
-    def hop_step(hop, carry):
-        arrive(hop)
-        pass_two(hop - 1)
-        sides(hop, lambda place, k: first_half(place))
-
-        @pl.when(hop == 2)
-        def _():
-            head_pass()
-
-        sides(hop - 1, lambda place, k: second_half(place, False))
-        pass_one(hop)
-        return carry
-
-    lax.fori_loop(2, chips, hop_step, 0)
-    pass_two(chips - 1)
-    sides(chips - 1, lambda place, k: second_half(place, False))
-    loads[8].wait()
-    head_wait()
-    mixer_out[...] = jnp.dot(heads[...], wo[...], preferred_element_type=jnp.float32).astype(
-        jnp.bfloat16
-    )
-
-    for k in range(1, chips):
-        source = lax.rem(z + k, chips)
-        result_copy(source, source).wait_recv()
-    total = returned[0].astype(jnp.float32)
-    for source in range(1, chips):
-        total += returned[source].astype(jnp.float32)
-    expert_out[...] = total.astype(jnp.bfloat16)
-
-    for place in range(chips):
+            action(unit(above, sub))
+
+    def deliver(u):
+        combine(u)
+        result_copy(u, z).start()
+
+    ending = lowest | highest
+    look = jnp.where(ending, EARLY, LATE)
+
+    def own_units(action):
+        for sub in range(SPLIT):
+            action(unit(z, sub))
+
+    def project():
+        head_wait()
+        mixer_out[...] = jnp.dot(heads[...], wo[...], preferred_element_type=jnp.float32).astype(
+            jnp.bfloat16
+        )
+
+    def drain(u, carry):
+        place, sub = u // SPLIT, u % SPLIT
+
         @pl.when((place <= z) & jnp.logical_not(highest))
         def _():
-            up_copy(place).wait_send()
+            up_copy(place, sub).wait_send()
 
         @pl.when((place >= z) & jnp.logical_not(lowest))
         def _():
-            down_copy(place).wait_send()
-
-        core_copy(place).wait_send()
-        half_copy(place).wait_send()
+            down_copy(place, sub).wait_send()
+
+        core_copy(place, sub).wait_send()
+        half_copy(u).wait_send()
         for k in direct:
             for half in range(2):
-                hidden_copy(tp, place, half, k).wait_send()
+                hidden_copy(tp, u, half, k).wait_send()
         if square:
             for way in range(2):
-                hidden_forward(place, way).wait_send()
+                hidden_forward(u, way).wait_send()
 
         @pl.when(place != z)
         def _():
-            result_copy(place, z).wait_send()
+            result_copy(u, z).wait_send()
+
+        return carry
+
+    units = chips * SPLIT
+
+    def step(index, carry):
+        hop, sub = 1 + index // SPLIT, index % SPLIT
+        arrive(hop, sub)
+        sides(hop, lambda place, k: first_half(unit(place, sub)))
+
+        @pl.when(index == 0)
+        def _():
+            for own_sub in range(1, SPLIT):
+                hidden_pass(unit(z, own_sub))
+
+        @pl.when(index > 0)
+        def _():
+            one(index - 1, hidden_pass)
+
+        @pl.when(index > 1)
+        def _():
+            two(index - 2, hidden_pass)
+
+        @pl.when((index >= look) & (index < look + 2))
+        def _():
+            attention(index - look)
+
+        @pl.when((index == 3) & ending)
+        def _():
+            head_pass()
+
+        @pl.when(index > 2)
+        def _():
+            one(index - 3, deliver)
+
+        @pl.when(index > 1)
+        def _():
+            one(index - 2, second_half)
+
+        @pl.when(index > 3)
+        def _():
+            two(index - 4, deliver)
+
+        @pl.when(index > 2)
+        def _():
+            two(index - 3, second_half)
+
+        return carry
+
+    loads[7].wait()
+    lax.fori_loop(0, n, spread_shares, 0)
+    hidden_pass(unit(z, 0))
+    lax.fori_loop(0, steps, step, 0)
+    loads[8].wait()
+    second_half(unit(z, 0))
+    one(steps - 1, hidden_pass)
+    two(steps - 2, hidden_pass)
+    two(steps - 1, hidden_pass)
+    one(steps - 3, deliver)
+    two(steps - 4, deliver)
+    for sub in range(1, SPLIT):
+        second_half(unit(z, sub))
+    one(steps - 2, second_half)
+    two(steps - 3, second_half)
+
+    @pl.when(ending)
+    def _():
+        project()
+
+    two(steps - 3, deliver)
+    one(steps - 2, deliver)
+    one(steps - 1, second_half)
+    two(steps - 2, second_half)
+    two(steps - 1, second_half)
+    one(steps - 1, deliver)
+    two(steps - 2, deliver)
+    two(steps - 1, deliver)
+
+    @pl.when(jnp.logical_not(ending))
+    def _():
+        head_pass()
+        project()
+
+    own_units(combine)
+    lax.fori_loop(0, units, drain, 0)
+
+    for sub in range(SPLIT):
+        total = result[unit(z, sub)].astype(jnp.float32)
+        for k in range(1, chips):
+            source = lax.rem(z + k, chips)
+            result_copy(unit(source, sub), source).wait_recv()
+            total += returned[source, sub].astype(jnp.float32)
+        expert_out[sub * size : (sub + 1) * size, :] = total.astype(jnp.bfloat16)
+
 
     for k in direct:
         for half in range(2):
@@ -644,6 +762,7 @@
     columns = down_weight.shape[2]
     spread = query_weight.shape[1]
     half = jnp.bfloat16
+    size, units = rows // SPLIT, chips * SPLIT
     return pl.pallas_call(
         functools.partial(exchange, experts, parts),
         out_shape=(
@@ -659,11 +778,14 @@
             pltpu.VMEM((experts * rows, parts * part), half),
             pltpu.VMEM((tokens, parts * spread), half),
             pltpu.VMEM((experts, experts, rows), jnp.float32),
-            pltpu.VMEM((chips, rows, columns), half),
-            pltpu.VMEM((chips, rows, columns), half),
-            pltpu.VMEM((chips, rows, columns), half),
-            pltpu.VMEM((chips, rows, columns), half),
-            pltpu.VMEM((rows, columns), jnp.float32),
+            pltpu.VMEM((units, size, columns), half),
+            pltpu.VMEM((units, size, columns), half),
+            pltpu.VMEM((units, size, columns), half),
+            pltpu.VMEM((chips, SPLIT, size, columns), half),
+            pltpu.VMEM((units, size, columns), jnp.float32),
+            pltpu.VMEM((experts * rows, rows), jnp.float32),
+            pltpu.VMEM((tokens, lanes), jnp.float32),
+            pltpu.VMEM((tokens, lanes), jnp.float32),
             pltpu.VMEM((tokens, spread), half),
             pltpu.VMEM((tokens + 2 * WINDOW, 2 * key_weight.shape[1]), half),
             pltpu.VMEM(query_weight.shape, half),
@@ -674,13 +796,13 @@
             pltpu.VMEM(up_weight.shape[1:], half),
             pltpu.VMEM(down_weight.shape[1:], half),
             dma((9,)),
-            dma((experts,)),
-            dma((chips,)),
-            dma((chips,)),
-            dma((chips,)),
-            dma((parts, chips, 2)),
-            dma((parts, chips, 2)),
-            dma((2, chips)),
+            dma((2 * units,)),
+            dma((units,)),
+            dma((units,)),
+            dma((units,)),
+            dma((parts, units, 2)),
+            dma((parts, units, 2)),
+            dma((2, units)),
             dma((parts, 2)),
             dma((parts, 2)),
             dma((2,)),
@@ -688,10 +810,10 @@
             dma((2,)),
             dma((experts,)),
             dma((experts,)),
-            dma((chips,)),
-            dma((chips,)),
-            dma((chips,)),
-            dma((chips,)),
+            dma((units,)),
+            dma((units,)),
+            dma((units,)),
+            dma((chips, SPLIT)),
         ],
         compiler_params=pltpu.CompilerParams(
             collective_id=0, has_side_effects=True, vmem_limit_bytes=60 * 1024 * 1024

time: 72.8 us -> 67.8 us (0.931)
  Pallas kernels: 68.7 us -> 63.7 us
    pallas_call x1, Pallas kernels: 68.7 us -> 63.7 us  [shards(): pl.pallas_call(functools.partial(exchange, experts, parts), out_shape=(ja...]
where the time goes in v2:
time: 67.8 us; the launch traced here: 67.6 us
  Pallas kernels  63.7 us (94%)
  local copies, waits for them, and re-layouts  3.24 us (5%)
    pallas_call x1, Pallas kernels, shards(): pl.pallas_call(functools.partial(exchange, experts, parts), out_shape=(ja...  63.7 us
    unnamed x2, local copies, waits for them, and re-layouts  3.24 us

profile of v2, /device:TPU:0, one launch (start us, length us, event | category | flops | bytes accessed | tf_op | source)
XLA Modules:
  0.0 67.6 jit_solution(9400160877194443940)
XLA Ops:
  0.6 63.7 %shard_map.158 = (bf16[256,512]{1,0:T(8,128)(2,1)}, bf16[128,512]{1,0:T(8,128)(2,1)}) custom-call(bf16[128,2048]{1,0:T(8,128)(2,1)} %x_hbm.1, f32[1,2048]{1,0:T(1,128)} %bitcast.11, f32[4,128]{1,0:T(4,128)} %bitcast.13, s32[4,128]{1,0:T(4,128)} %bitcast.14, bf16[256,2048]{1,0:T(8,128)(2,1)} %mixer_hbm.1, f32[1,2048]{1,0:T(1,128)} %bitcast.12, ...), custom_call_target="tpu_custom_call" | custom-call | tf_op jit(solution)/shard_map/pallas_call | solution.py:766
  64.4 1.7 %copy.19 = bf16[256,512]{1,0:T(8,128)(2,1)} copy(bf16[256,512]{1,0:T(8,128)(2,1)} %get-tuple-element.4) | data formatting | bytes 524288
  66.1 1.6 %copy.20 = bf16[128,512]{1,0:T(8,128)(2,1)} copy(bf16[128,512]{1,0:T(8,128)(2,1)} %get-tuple-element.5) | data formatting | bytes 262144

commit v3 on v2

--- a/solution.py
+++ b/solution.py
@@ -69,13 +69,13 @@
     n,
     t,
     x_hbm,
-    gain_ref,
-    logit_ref,
-    route_ref,
+    gain_hbm,
+    logit_hbm,
+    route_hbm,
     mixer_hbm,
-    mixer_gain_ref,
-    frequency_ref,
-    sink_ref,
+    mixer_gain_hbm,
+    frequency_hbm,
+    sink_hbm,
     wq_hbm,
     wk_hbm,
     wv_hbm,
@@ -85,6 +85,12 @@
     wd_hbm,
     mixer_out,
     expert_out,
+    gain_ref,
+    logit_ref,
+    route_ref,
+    mixer_gain_ref,
+    frequency_ref,
+    sink_ref,
     x_ref,
     mixer_ref,
     tokens,
@@ -162,9 +168,15 @@
             (wq_hbm, wq),
             (wd_hbm, wd),
             (wo_hbm, wo),
+            (frequency_hbm, frequency_ref),
+            (logit_hbm, logit_ref),
+            (route_hbm, route_ref),
+            (gain_hbm, gain_ref),
+            (mixer_gain_hbm, mixer_gain_ref),
+            (sink_hbm, sink_ref),
         ))
     ]
-    for load in loads:
+    for load in loads[9:] + loads[:9]:
         load.start()
 
     barrier = pltpu.get_barrier_semaphore()
@@ -183,6 +195,8 @@
             device_id_type=pl.DeviceIdType.MESH,
         )
 
+    for load in loads[9:]:
+        load.wait()
     logits = logit_ref[...]
     raised = jnp.exp(logits - jnp.max(logits, axis=0, keepdims=True))
     chances = raised / jnp.sum(raised, axis=0, keepdims=True)
@@ -223,7 +237,7 @@
 
     def core_copy(place, sub):
         u = unit(place, sub)
-        return token_copy(2 * u + core, core_send.at[u], partner)
+        return token_copy(2 * u + core, core_send.at[0], partner)
 
     def token_wait(slot):
         token_copy(slot, core_send.at[0], partner).wait_recv()
@@ -231,7 +245,7 @@
     def share_copy(k):
         piece = shares.at[ep]
         target = lax.rem(ep + k, n)
-        return remote(piece, piece, share_send.at[k], share_recv.at[ep], target, tp)
+        return remote(piece, piece, share_send.at[0], share_recv.at[ep], target, tp)
 
     def share_wait(slot):
         piece = shares.at[slot]
@@ -258,7 +272,7 @@
         return remote(
             piece,
             piece,
-            hidden_send.at[k, u, half],
+            hidden_send.at[k],
             hidden_recv.at[source, u, half],
             ep,
             peer(k),
@@ -270,7 +284,7 @@
         return remote(
             piece,
             piece,
-            pass_send.at[way, u],
+            pass_send.at[way],
             hidden_recv.at[source, u, 1 - way],
             ep,
             peer(1 + way),
@@ -297,7 +311,7 @@
     def head_copy(source, half, k):
         piece = head_piece(source, half)
         return remote(
-            piece, piece, head_send.at[k, half], head_recv.at[source, half], ep, peer(k)
+            piece, piece, head_send.at[k], head_recv.at[source, half], ep, peer(k)
         )
 
     def head_forward(way):
@@ -351,15 +365,15 @@
             for k in direct:
                 hidden_copy(tp, unit(z, sub), side, k).start()
 
-    loads[1].wait()
-    loads[2].wait()
-    first_own(core)
     pl.semaphore_wait(barrier, n + t - 2)
     for k in range(1, n):
         share_copy(k).start()
     spread_own(0)
     for sub in range(SPLIT):
         core_copy(z, sub).start()
+    loads[1].wait()
+    loads[2].wait()
+    first_own(core)
     send_own(core)
 
     loads[3].wait()
@@ -479,14 +493,14 @@
 
     def half_copy(u):
         return remote(
-            half_out.at[u], half_in.at[u], half_send.at[u], half_recv.at[u], partner, tp
+            half_out.at[u], half_in.at[u], half_send.at[0], half_recv.at[u], partner, tp
         )
 
     def result_copy(u, source):
         return remote(
             result.at[u],
             returned.at[source, u % SPLIT],
-            result_send.at[u],
+            result_send.at[0],
             result_recv.at[source, u % SPLIT],
             2 * (u // SPLIT) + core,
             tp,
@@ -504,23 +518,20 @@
             scales[inside, :] = column[sub * size : (sub + 1) * size]
         return carry
 
-    def scaled(slot):
-        inside = block(slot, size)
+    def second_half(u):
+        hidden_wait(u)
+        inside = block(u, pair)
         total = jnp.dot(hidden[inside, :], wd[...], preferred_element_type=jnp.float32)
         column = scales[inside, :]
-        return jnp.concatenate(
+        kept_half[u] = jnp.concatenate(
             [total[:, i : i + rows] * column for i in range(0, total.shape[1], rows)], axis=1
         )
-
-    def second_half(u):
-        hidden_wait(u)
-        half_out[u] = scaled(2 * u + 1 - core).astype(jnp.bfloat16)
+        half_out[u] = kept_half[u, block(1 - core, size), :].astype(jnp.bfloat16)
         half_copy(u).start()
-        kept_half[u] = scaled(2 * u + core)
 
     def combine(u):
         half_copy(u).wait_recv()
-        total = kept_half[u] + half_in[u].astype(jnp.float32)
+        total = kept_half[u, block(core, size), :] + half_in[u].astype(jnp.float32)
         result[u] = total.astype(jnp.bfloat16)
 
     def sides(hop, action):
@@ -604,20 +615,36 @@
         def _():
             down_copy(place, sub).wait_send()
 
-        core_copy(place, sub).wait_send()
-        half_copy(u).wait_send()
+        return carry
+
+    def drain_all():
+        lax.fori_loop(0, units, drain, 0)
+
+        def sent(view, semaphore):
+            remote(view, view, semaphore, semaphore, partner, tp).wait_send()
+
+        def column(buffer, count, extent):
+            return buffer.at[pl.ds(0, count), pl.ds(0, extent)]
+
+        sent(tokens.at[pl.ds(0, rows * chips)], core_send.at[0])
+        sent(half_out, half_send.at[0])
+        sent(result.at[pl.ds(0, units - SPLIT)], result_send.at[0])
+        sent(shares.at[pl.ds(0, n - 1)], share_send.at[0])
         for k in direct:
-            for half in range(2):
-                hidden_copy(tp, u, half, k).wait_send()
+            sent(column(hidden, n * rows, part), hidden_send.at[k])
+            sent(column(heads, length, spread), head_send.at[k])
         if square:
             for way in range(2):
-                hidden_forward(u, way).wait_send()
-
-        @pl.when(place != z)
-        def _():
-            result_copy(u, z).wait_send()
-
-        return carry
+                sent(column(hidden, chips * rows, part), pass_send.at[way])
+                head_forward(way).wait_send()
+
+        @pl.when(jnp.logical_not(last))
+        def _():
+            edge_copy(0).wait_send()
+
+        @pl.when(jnp.logical_not(first))
+        def _():
+            edge_copy(1).wait_send()
 
     units = chips * SPLIT
 
@@ -700,7 +727,7 @@
         project()
 
     own_units(combine)
-    lax.fori_loop(0, units, drain, 0)
+    drain_all()
 
     for sub in range(SPLIT):
         total = result[unit(z, sub)].astype(jnp.float32)
@@ -711,23 +738,9 @@
         expert_out[sub * size : (sub + 1) * size, :] = total.astype(jnp.bfloat16)
 
 
-    for k in direct:
-        for half in range(2):
-            head_copy(tp, half, k).wait_send()
-    if square:
-        for way in range(2):
-            head_forward(way).wait_send()
-
-    @pl.when(jnp.logical_not(last))
-    def _():
-        edge_copy(0).wait_send()
-
-    @pl.when(jnp.logical_not(first))
-    def _():
-        edge_copy(1).wait_send()
-
-    for k in range(1, n):
-        share_copy(k).wait_send()
+def settle(first_ref, second_ref, first_out, second_out):
+    first_out[...] = first_ref[...]
+    second_out[...] = second_ref[...]
 
 
 def shards(
@@ -756,22 +769,28 @@
     rows, width = expert_input.shape
     part = gate_weight.shape[2]
     vmem = pl.BlockSpec(memory_space=pltpu.VMEM)
-    anywhere = pl.BlockSpec(memory_space=pl.ANY)
+    outside = pl.BlockSpec(memory_space=pltpu.HBM)
     chips = experts // 2
     dma = pltpu.SemaphoreType.DMA
     columns = down_weight.shape[2]
     spread = query_weight.shape[1]
     half = jnp.bfloat16
     size, units = rows // SPLIT, chips * SPLIT
-    return pl.pallas_call(
+    results = pl.pallas_call(
         functools.partial(exchange, experts, parts),
         out_shape=(
             jax.ShapeDtypeStruct((tokens, output_weight.shape[1]), half),
             jax.ShapeDtypeStruct((rows, columns), half),
         ),
-        in_specs=[anywhere, vmem, vmem, vmem, anywhere, vmem, vmem, vmem] + [anywhere] * 7,
+        in_specs=[outside] * 15,
         out_specs=(vmem, vmem),
         scratch_shapes=[
+            pltpu.VMEM((1, width), jnp.float32),
+            pltpu.VMEM((TOP_K, rows), jnp.float32),
+            pltpu.VMEM((TOP_K, rows), jnp.int32),
+            pltpu.VMEM((1, width), jnp.float32),
+            pltpu.VMEM((1, lanes), jnp.float32),
+            pltpu.VMEM((1, sink_logit.shape[0]), jnp.float32),
             pltpu.VMEM((rows, width), half),
             pltpu.VMEM(mixer_input.shape, half),
             pltpu.VMEM((experts * rows, width), half),
@@ -782,7 +801,7 @@
             pltpu.VMEM((units, size, columns), half),
             pltpu.VMEM((units, size, columns), half),
             pltpu.VMEM((chips, SPLIT, size, columns), half),
-            pltpu.VMEM((units, size, columns), jnp.float32),
+            pltpu.VMEM((units, 2 * size, columns), jnp.float32),
             pltpu.VMEM((experts * rows, rows), jnp.float32),
             pltpu.VMEM((tokens, lanes), jnp.float32),
             pltpu.VMEM((tokens, lanes), jnp.float32),
@@ -795,24 +814,24 @@
             pltpu.VMEM(gate_weight.shape[1:], half),
             pltpu.VMEM(up_weight.shape[1:], half),
             pltpu.VMEM(down_weight.shape[1:], half),
-            dma((9,)),
+            dma((15,)),
             dma((2 * units,)),
             dma((units,)),
             dma((units,)),
-            dma((units,)),
+            dma((1,)),
+            dma((parts,)),
             dma((parts, units, 2)),
-            dma((parts, units, 2)),
-            dma((2, units)),
-            dma((parts, 2)),
+            dma((2,)),
+            dma((parts,)),
             dma((parts, 2)),
             dma((2,)),
             dma((2,)),
             dma((2,)),
+            dma((1,)),
             dma((experts,)),
-            dma((experts,)),
+            dma((1,)),
             dma((units,)),
-            dma((units,)),
-            dma((units,)),
+            dma((1,)),
             dma((chips, SPLIT)),
         ],
         compiler_params=pltpu.CompilerParams(
@@ -835,6 +854,12 @@
         up_weight[0],
         down_weight[0],
     )
+    return pl.pallas_call(
+        settle,
+        out_shape=tuple(jax.ShapeDtypeStruct(r.shape, r.dtype) for r in results),
+        in_specs=[vmem, vmem],
+        out_specs=(vmem, vmem),
+    )(*results)
 
 
 def solution(mesh):

time: 67.8 us -> 63.7 us (0.940)
  local copies, waits for them, and re-layouts: 3.24 us -> 0 us
  Pallas kernels: 63.7 us -> 62.9 us
    unnamed x2 -> x0, local copies, waits for them, and re-layouts: 3.24 us -> none
    pallas_call x1, Pallas kernels: 63.7 us -> 61.2 us  [shards(): pl.pallas_call(functools.partial(exchange, experts, parts), out_shape=(ja...]
    pallas_call x0 -> x1, Pallas kernels: none -> 1.74 us  [shards(): pl.pallas_call(settle, out_shape=tuple((jax.ShapeDtypeStruct(r.shape, r.d...]
where the time goes in v3:
time: 63.7 us; the launch traced here: 63.6 us
  Pallas kernels  62.9 us (99%)
  between operations  0.64 us (1%)
    pallas_call x1, Pallas kernels, shards(): pl.pallas_call(functools.partial(exchange, experts, parts), out_shape=(ja...  61.2 us
    pallas_call x1, Pallas kernels, shards(): pl.pallas_call(settle, out_shape=tuple((jax.ShapeDtypeStruct(r.shape, r.d...  1.74 us

profile of v3, /device:TPU:0, one launch (start us, length us, event | category | flops | bytes accessed | tf_op | source)
XLA Modules:
  0.0 63.6 jit_solution(2870358412388005258)
XLA Ops:
  0.6 61.2 %shard_map.158 = (bf16[256,512]{1,0:T(8,128)(2,1)}, bf16[128,512]{1,0:T(8,128)(2,1)}) custom-call(bf16[128,2048]{1,0:T(8,128)(2,1)} %x_hbm.1, f32[1,2048]{1,0:T(1,128)} %bitcast.11, f32[4,128]{1,0:T(4,128)} %bitcast.13, s32[4,128]{1,0:T(4,128)} %bitcast.14, bf16[256,2048]{1,0:T(8,128)(2,1)} %mixer_hbm.1, f32[1,2048]{1,0:T(1,128)} %bitcast.12, ...), custom_call_target="tpu_custom_call" | custom-call | tf_op jit(solution)/shard_map/pallas_call | solution.py:779
  61.8 1.7 %shard_map.159 = (bf16[256,512]{1,0:T(8,128)(2,1)}, bf16[128,512]{1,0:T(8,128)(2,1)}) custom-call(bf16[256,512]{1,0:T(8,128)(2,1)} %get-tuple-element.4.first_ref, bf16[128,512]{1,0:T(8,128)(2,1)} %get-tuple-element.5.second_ref), custom_call_target="tpu_custom_call" | custom-call | tf_op jit(solution)/shard_map/pallas_call | solution.py:857

commit v4 on v3

--- a/solution.py
+++ b/solution.py
@@ -83,6 +83,8 @@
     wg_hbm,
     wu_hbm,
     wd_hbm,
+    mixer_hbm_out,
+    expert_hbm_out,
     mixer_out,
     expert_out,
     gain_ref,
@@ -105,6 +107,7 @@
     scales,
     cosine_ref,
     sine_ref,
+    lent,
     queries,
     around,
     wq,
@@ -115,6 +118,7 @@
     wu,
     wd,
     local_sem,
+    out_sem,
     token_recv,
     up_send,
     down_send,
@@ -127,6 +131,8 @@
     head_pass_send,
     edge_send,
     edge_recv,
+    lent_send,
+    lent_recv,
     share_send,
     share_recv,
     half_send,
@@ -245,11 +251,11 @@
     def share_copy(k):
         piece = shares.at[ep]
         target = lax.rem(ep + k, n)
-        return remote(piece, piece, share_send.at[0], share_recv.at[ep], target, tp)
-
-    def share_wait(slot):
-        piece = shares.at[slot]
-        remote(piece, piece, share_send.at[0], share_recv.at[slot], partner, tp).wait_recv()
+        return remote(piece, piece, share_send.at[0], share_recv.at[0], target, tp)
+
+    def share_wait():
+        piece = shares.at[pl.ds(0, n - 1)]
+        remote(piece, piece, share_send.at[0], share_recv.at[0], partner, tp).wait_recv()
 
     lowest, highest = z == 0, z == chips - 1
 
@@ -266,6 +272,11 @@
         return hidden.at[
             block(2 * u + half, size), pl.ds(pl.multiple_of(source * part, part), part)
         ]
+
+    def kind_of(k, half):
+        if square and k < 3:
+            return jnp.where(half == k - 1, k - 1, 2)
+        return 2
 
     def hidden_copy(source, u, half, k):
         piece = hidden_piece(source, u, half)
@@ -273,7 +284,7 @@
             piece,
             piece,
             hidden_send.at[k],
-            hidden_recv.at[source, u, half],
+            hidden_recv.at[u, kind_of(k, half)],
             ep,
             peer(k),
         )
@@ -285,7 +296,7 @@
             piece,
             piece,
             pass_send.at[way],
-            hidden_recv.at[source, u, 1 - way],
+            hidden_recv.at[u, 2],
             ep,
             peer(1 + way),
         )
@@ -296,11 +307,11 @@
                 hidden_copy(peer(2 - way), u, 1 - way, 2 - way).wait_recv()
                 hidden_forward(u, way).start()
 
+    others = 2 if square else t - 1
+
     def hidden_wait(u):
-        for k in range(1, t):
-            for half in range(2):
-                if not (square and (k, half) in ((1, 0), (2, 1))):
-                    hidden_copy(peer(k), u, half, direct[0]).wait_recv()
+        view = hidden.at[pl.ds(0, pair), pl.ds(0, others * part)]
+        remote(view, view, hidden_send.at[0], hidden_recv.at[u, 2], ep, peer(1)).wait_recv()
 
     def head_piece(source, half):
         return heads.at[
@@ -311,7 +322,7 @@
     def head_copy(source, half, k):
         piece = head_piece(source, half)
         return remote(
-            piece, piece, head_send.at[k], head_recv.at[source, half], ep, peer(k)
+            piece, piece, head_send.at[k], head_recv.at[kind_of(k, half)], ep, peer(k)
         )
 
     def head_forward(way):
@@ -321,7 +332,7 @@
             piece,
             piece,
             head_pass_send.at[way],
-            head_recv.at[source, 1 - way],
+            head_recv.at[2],
             ep,
             peer(1 + way),
         )
@@ -333,10 +344,8 @@
                 head_forward(way).start()
 
     def head_wait():
-        for k in range(1, t):
-            for half in range(2):
-                if not (square and (k, half) in ((1, 0), (2, 1))):
-                    head_copy(peer(k), half, direct[0]).wait_recv()
+        view = heads.at[:, pl.ds(0, others * spread)]
+        remote(view, view, head_send.at[0], head_recv.at[2], ep, peer(1)).wait_recv()
 
     def expand(slots):
         span = min(256, part)
@@ -388,26 +397,55 @@
         jnp.bfloat16
     )
 
-    def edge_copy(way):
+    reach = WINDOW // 2
+
+    def edge_copy(way, part_of):
         source, target = (length, 0) if way == 0 else (WINDOW, WINDOW + length)
         return remote(
-            around.at[pl.ds(source, WINDOW)],
-            around.at[pl.ds(target, WINDOW)],
-            edge_send.at[way],
-            edge_recv.at[way],
+            around.at[pl.ds(source + part_of * reach, reach)],
+            around.at[pl.ds(target + part_of * reach, reach)],
+            edge_send.at[way, part_of],
+            edge_recv.at[way, part_of],
             ep + (1 if way == 0 else -1),
             tp,
         )
 
+    def lend_copy(way):
+        source = length if way == 0 else WINDOW
+        return remote(
+            around.at[pl.ds(source + reach, reach)],
+            lent,
+            edge_send.at[way, 1],
+            lent_recv.at[0],
+            partner,
+            tp,
+        )
+
+    def lent_copy(way):
+        target = 0 if way == 0 else WINDOW + length
+        return remote(
+            lent,
+            around.at[pl.ds(target + reach, reach)],
+            lent_send.at[0],
+            edge_recv.at[way, 1],
+            partner + (1 if way == 0 else -1),
+            tp,
+        )
+
     first, last = ep == 0, ep == n - 1
 
-    @pl.when(jnp.logical_not(last))
-    def _():
-        edge_copy(0).start()
-
-    @pl.when(jnp.logical_not(first))
-    def _():
-        edge_copy(1).start()
+    crossing = ((core == 1) & jnp.logical_not(highest), (core == 0) & jnp.logical_not(lowest))
+    lending = ((core == 0) & jnp.logical_not(highest), (core == 1) & jnp.logical_not(lowest))
+    for way in range(2):
+        @pl.when(core == way)
+        def _():
+            for part_of in range(2):
+                edge_copy(way, part_of).start()
+
+        @pl.when(crossing[way])
+        def _():
+            lend_copy(way).start()
+            edge_copy(way, 0).start()
 
     for sub in range(1, SPLIT):
         spread_own(sub)
@@ -424,6 +462,12 @@
         token_wait(2 * unit(z, sub) + 1 - core)
     first_own(1 - core)
     send_own(1 - core)
+
+    for way in range(2):
+        @pl.when(lending[way])
+        def _():
+            lend_copy(way).wait_recv()
+            lent_copy(way).start()
 
     loads[6].wait()
     turned = jnp.dot(normed, wq[...], preferred_element_type=jnp.float32)
@@ -478,13 +522,11 @@
         return carry
 
     def attention(half):
-        @pl.when((half == 0) & jnp.logical_not(first))
-        def _():
-            edge_copy(0).wait_recv()
-
-        @pl.when((half == 1) & jnp.logical_not(last))
-        def _():
-            edge_copy(1).wait_recv()
+        for way in range(2):
+            @pl.when((half == way) & jnp.logical_not(first if way == 0 else last))
+            def _():
+                for part_of in range(2):
+                    edge_copy(way, part_of).wait_recv()
 
         count = length // 2 // WINDOW
         lax.fori_loop(half * count, (half + 1) * count, attend, 0)
@@ -501,16 +543,12 @@
             result.at[u],
             returned.at[source, u % SPLIT],
             result_send.at[0],
-            result_recv.at[source, u % SPLIT],
+            result_recv.at[u % SPLIT],
             2 * (u // SPLIT) + core,
             tp,
         )
 
     def spread_shares(slot, carry):
-        @pl.when(slot != ep)
-        def _():
-            share_wait(slot)
-
         line = shares[slot, pl.ds(ep, 1), :]
         column = jnp.transpose(jnp.broadcast_to(line, (rows, rows)))
         for sub in range(SPLIT):
@@ -598,11 +636,18 @@
         for sub in range(SPLIT):
             action(unit(z, sub))
 
+    mixer_store = pltpu.make_async_copy(mixer_out, mixer_hbm_out, out_sem.at[SPLIT])
+
+    def expert_store(sub):
+        inside = pl.ds(sub * size, size)
+        return pltpu.make_async_copy(expert_out.at[inside], expert_hbm_out.at[inside], out_sem.at[sub])
+
     def project():
         head_wait()
         mixer_out[...] = jnp.dot(heads[...], wo[...], preferred_element_type=jnp.float32).astype(
             jnp.bfloat16
         )
+        mixer_store.start()
 
     def drain(u, carry):
         place, sub = u // SPLIT, u % SPLIT
@@ -638,13 +683,15 @@
                 sent(column(hidden, chips * rows, part), pass_send.at[way])
                 head_forward(way).wait_send()
 
-        @pl.when(jnp.logical_not(last))
-        def _():
-            edge_copy(0).wait_send()
-
-        @pl.when(jnp.logical_not(first))
-        def _():
-            edge_copy(1).wait_send()
+        for way in range(2):
+            @pl.when((core == way) | crossing[way])
+            def _():
+                for part_of in range(2):
+                    edge_copy(way, part_of).wait_send()
+
+            @pl.when(lending[way])
+            def _():
+                lent_copy(way).wait_send()
 
     units = chips * SPLIT
 
@@ -668,7 +715,7 @@
 
         @pl.when((index >= look) & (index < look + 2))
         def _():
-            attention(index - look)
+            attention(jnp.where(highest, 1 - (index - look), index - look))
 
         @pl.when((index == 3) & ending)
         def _():
@@ -693,6 +740,7 @@
         return carry
 
     loads[7].wait()
+    share_wait()
     lax.fori_loop(0, n, spread_shares, 0)
     hidden_pass(unit(z, 0))
     lax.fori_loop(0, steps, step, 0)
@@ -701,19 +749,19 @@
     one(steps - 1, hidden_pass)
     two(steps - 2, hidden_pass)
     two(steps - 1, hidden_pass)
+    for sub in range(1, SPLIT):
+        second_half(unit(z, sub))
     one(steps - 3, deliver)
     two(steps - 4, deliver)
-    for sub in range(1, SPLIT):
-        second_half(unit(z, sub))
-    one(steps - 2, second_half)
-    two(steps - 3, second_half)
-
     @pl.when(ending)
     def _():
         project()
 
+    one(steps - 2, second_half)
+    two(steps - 3, second_half)
+    one(steps - 2, deliver)
     two(steps - 3, deliver)
-    one(steps - 2, deliver)
+
     one(steps - 1, second_half)
     two(steps - 2, second_half)
     two(steps - 1, second_half)
@@ -731,11 +779,17 @@
 
     for sub in range(SPLIT):
         total = result[unit(z, sub)].astype(jnp.float32)
+        view = result.at[pl.ds(0, chips - 1)]
+        remote(view, view, result_send.at[0], result_recv.at[sub], partner, tp).wait_recv()
         for k in range(1, chips):
             source = lax.rem(z + k, chips)
-            result_copy(unit(source, sub), source).wait_recv()
             total += returned[source, sub].astype(jnp.float32)
         expert_out[sub * size : (sub + 1) * size, :] = total.astype(jnp.bfloat16)
+        expert_store(sub).start()
+
+    for sub in range(SPLIT):
+        expert_store(sub).wait()
+    mixer_store.wait()
 
 
 def settle(first_ref, second_ref, first_out, second_out):
@@ -783,8 +837,10 @@
             jax.ShapeDtypeStruct((rows, columns), half),
         ),
         in_specs=[outside] * 15,
-        out_specs=(vmem, vmem),
+        out_specs=(outside, outside),
         scratch_shapes=[
+            pltpu.VMEM((tokens, output_weight.shape[1]), half),
+            pltpu.VMEM((rows, columns), half),
             pltpu.VMEM((1, width), jnp.float32),
             pltpu.VMEM((TOP_K, rows), jnp.float32),
             pltpu.VMEM((TOP_K, rows), jnp.int32),
@@ -805,6 +861,7 @@
             pltpu.VMEM((experts * rows, rows), jnp.float32),
             pltpu.VMEM((tokens, lanes), jnp.float32),
             pltpu.VMEM((tokens, lanes), jnp.float32),
+            pltpu.VMEM((WINDOW // 2, 2 * key_weight.shape[1]), half),
             pltpu.VMEM((tokens, spread), half),
             pltpu.VMEM((tokens + 2 * WINDOW, 2 * key_weight.shape[1]), half),
             pltpu.VMEM(query_weight.shape, half),
@@ -815,24 +872,27 @@
             pltpu.VMEM(up_weight.shape[1:], half),
             pltpu.VMEM(down_weight.shape[1:], half),
             dma((15,)),
+            dma((SPLIT + 1,)),
             dma((2 * units,)),
             dma((units,)),
             dma((units,)),
             dma((1,)),
             dma((parts,)),
-            dma((parts, units, 2)),
+            dma((units, 3)),
             dma((2,)),
             dma((parts,)),
-            dma((parts, 2)),
+            dma((3,)),
             dma((2,)),
-            dma((2,)),
-            dma((2,)),
+            dma((2, 2)),
+            dma((2, 2)),
             dma((1,)),
-            dma((experts,)),
+            dma((1,)),
+            dma((1,)),
+            dma((1,)),
             dma((1,)),
             dma((units,)),
             dma((1,)),
-            dma((chips, SPLIT)),
+            dma((SPLIT,)),
         ],
         compiler_params=pltpu.CompilerParams(
             collective_id=0, has_side_effects=True, vmem_limit_bytes=60 * 1024 * 1024

time: 63.7 us -> 62.7 us (0.984)
  Pallas kernels: 62.9 us -> 61.9 us
    pallas_call x1, Pallas kernels: 61.2 us -> 60.2 us  [shards(): pl.pallas_call(functools.partial(exchange, experts, parts), out_shape=(ja...]
where the time goes in v4:
time: 62.7 us; the launch traced here: 62.6 us
  Pallas kernels  61.9 us (99%)
  between operations  0.64 us (1%)
    pallas_call x1, Pallas kernels, shards(): pl.pallas_call(functools.partial(exchange, experts, parts), out_shape=(ja...  60.2 us
    pallas_call x1, Pallas kernels, shards(): pl.pallas_call(settle, out_shape=tuple((jax.ShapeDtypeStruct(r.shape, r.d...  1.74 us

profile of v4, /device:TPU:0, one launch (start us, length us, event | category | flops | bytes accessed | tf_op | source)
XLA Modules:
  0.0 62.6 jit_solution(16458118287330949719)
XLA Ops:
  0.6 60.2 %shard_map.158 = (bf16[256,512]{1,0:T(8,128)(2,1)}, bf16[128,512]{1,0:T(8,128)(2,1)}) custom-call(bf16[128,2048]{1,0:T(8,128)(2,1)} %x_hbm.1, f32[1,2048]{1,0:T(1,128)} %bitcast.11, f32[4,128]{1,0:T(4,128)} %bitcast.13, s32[4,128]{1,0:T(4,128)} %bitcast.14, bf16[256,2048]{1,0:T(8,128)(2,1)} %mixer_hbm.1, f32[1,2048]{1,0:T(1,128)} %bitcast.12, ...), custom_call_target="tpu_custom_call" | custom-call | tf_op jit(solution)/shard_map/pallas_call | solution.py:833
  60.8 1.7 %shard_map.159 = (bf16[256,512]{1,0:T(8,128)(2,1)}, bf16[128,512]{1,0:T(8,128)(2,1)}) custom-call(bf16[256,512]{1,0:T(8,128)(2,1)} %get-tuple-element.4.first_ref, bf16[128,512]{1,0:T(8,128)(2,1)} %get-tuple-element.5.second_ref), custom_call_target="tpu_custom_call" | custom-call | tf_op jit(solution)/shard_map/pallas_call | solution.py:917

commit v5 on v4

--- a/solution.py
+++ b/solution.py
@@ -662,19 +662,29 @@
 
         return carry
 
-    def drain_all():
+    def sent(view, semaphore):
+        remote(view, view, semaphore, semaphore, partner, tp).wait_send()
+
+    def column(buffer, count, extent):
+        return buffer.at[pl.ds(0, count), pl.ds(0, extent)]
+
+    def drain_early():
         lax.fori_loop(0, units, drain, 0)
-
-        def sent(view, semaphore):
-            remote(view, view, semaphore, semaphore, partner, tp).wait_send()
-
-        def column(buffer, count, extent):
-            return buffer.at[pl.ds(0, count), pl.ds(0, extent)]
-
         sent(tokens.at[pl.ds(0, rows * chips)], core_send.at[0])
+        sent(shares.at[pl.ds(0, n - 1)], share_send.at[0])
+        for way in range(2):
+            @pl.when((core == way) | crossing[way])
+            def _():
+                for part_of in range(2):
+                    edge_copy(way, part_of).wait_send()
+
+            @pl.when(lending[way])
+            def _():
+                lent_copy(way).wait_send()
+
+    def drain_late():
         sent(half_out, half_send.at[0])
         sent(result.at[pl.ds(0, units - SPLIT)], result_send.at[0])
-        sent(shares.at[pl.ds(0, n - 1)], share_send.at[0])
         for k in direct:
             sent(column(hidden, n * rows, part), hidden_send.at[k])
             sent(column(heads, length, spread), head_send.at[k])
@@ -682,16 +692,6 @@
             for way in range(2):
                 sent(column(hidden, chips * rows, part), pass_send.at[way])
                 head_forward(way).wait_send()
-
-        for way in range(2):
-            @pl.when((core == way) | crossing[way])
-            def _():
-                for part_of in range(2):
-                    edge_copy(way, part_of).wait_send()
-
-            @pl.when(lending[way])
-            def _():
-                lent_copy(way).wait_send()
 
     units = chips * SPLIT
 
@@ -757,6 +757,7 @@
     def _():
         project()
 
+    drain_early()
     one(steps - 2, second_half)
     two(steps - 3, second_half)
     one(steps - 2, deliver)
@@ -775,7 +776,7 @@
         project()
 
     own_units(combine)
-    drain_all()
+    drain_late()
 
     for sub in range(SPLIT):
         total = result[unit(z, sub)].astype(jnp.float32)
@@ -792,9 +793,22 @@
     mixer_store.wait()
 
 
-def settle(first_ref, second_ref, first_out, second_out):
-    first_out[...] = first_ref[...]
-    second_out[...] = second_ref[...]
+def settle(first_in, second_in, first_out, second_out, first, second, semaphore):
+    taken = [
+        pltpu.make_async_copy(a, b, semaphore.at[i])
+        for i, (a, b) in enumerate(((first_in, first), (second_in, second)))
+    ]
+    given = [
+        pltpu.make_async_copy(a, b, semaphore.at[2 + i])
+        for i, (a, b) in enumerate(((first, first_out), (second, second_out)))
+    ]
+    for copy in taken:
+        copy.start()
+    for i in (1, 0):
+        taken[i].wait()
+        given[i].start()
+    for copy in given:
+        copy.wait()
 
 
 def shards(
@@ -917,8 +931,9 @@
     return pl.pallas_call(
         settle,
         out_shape=tuple(jax.ShapeDtypeStruct(r.shape, r.dtype) for r in results),
-        in_specs=[vmem, vmem],
-        out_specs=(vmem, vmem),
+        in_specs=[outside, outside],
+        out_specs=(outside, outside),
+        scratch_shapes=[pltpu.VMEM(r.shape, r.dtype) for r in results] + [dma((4,))],
     )(*results)
 
 

time: 62.7 us -> 62.7 us (level)
  no operation moved by 1% of the time
where the time goes in v5:
time: 62.7 us; the launch traced here: 62.6 us
  Pallas kernels  61.9 us (99%)
  between operations  0.64 us (1%)
    pallas_call x1, Pallas kernels, shards(): pl.pallas_call(functools.partial(exchange, experts, parts), out_shape=(ja...  60.2 us
    pallas_call x1, Pallas kernels, shards(): pl.pallas_call(settle, out_shape=tuple((jax.ShapeDtypeStruct(r.shape, r.d...  1.76 us

profile of v5, /device:TPU:0, one launch (start us, length us, event | category | flops | bytes accessed | tf_op | source)
XLA Modules:
  0.0 62.6 jit_solution(188364929355765389)
XLA Ops:
  0.6 60.2 %shard_map.158 = (bf16[256,512]{1,0:T(8,128)(2,1)}, bf16[128,512]{1,0:T(8,128)(2,1)}) custom-call(bf16[128,2048]{1,0:T(8,128)(2,1)} %x_hbm.1, f32[1,2048]{1,0:T(1,128)} %bitcast.11, f32[4,128]{1,0:T(4,128)} %bitcast.13, s32[4,128]{1,0:T(4,128)} %bitcast.14, bf16[256,2048]{1,0:T(8,128)(2,1)} %mixer_hbm.1, f32[1,2048]{1,0:T(1,128)} %bitcast.12, ...), custom_call_target="tpu_custom_call" | custom-call | tf_op jit(solution)/shard_map/pallas_call | solution.py:847
  60.8 1.8 %shard_map.159 = (bf16[256,512]{1,0:T(8,128)(2,1)}, bf16[128,512]{1,0:T(8,128)(2,1)}) custom-call(bf16[256,512]{1,0:T(8,128)(2,1)} %get-tuple-element.4.first_in, bf16[128,512]{1,0:T(8,128)(2,1)} %get-tuple-element.5.second_in), custom_call_target="tpu_custom_call" | custom-call | tf_op jit(solution)/shard_map/pallas_call | solution.py:931
